TPU v7x, 128 devices: a whole 4x4x4 slice. The times are simulated.
128 devices in a mesh: sp: 32 (over z, y, core), tp: 4 (over x).
Axes of the slice: x: 4, y: 4, z: 4, core: 2. Of those that a mesh axis runs over, the one named last changes fastest.
Arguments:
- mixer_value_projection: bfloat16 [24576, 2048], P('sp', 'tp'), may hold values from -6 to 6
- write_vectors_projected: bfloat16 [24576, 256], P('sp', 'tp'), may hold values from -6 to 6
- read_vectors_projected: bfloat16 [24576, 256], P('sp', 'tp'), may hold values from -6 to 6
- output_gate_projected: bfloat16 [24576, 2048], P('sp', 'tp'), may hold values from -6 to 6
- step_size_scores: float32 [24576, 32], P('sp', 'tp'), may hold values from -8 to 8
- position_decay_extra: float32 [24576, 32], P('sp', 'tp'), may hold values from -1 to 0
- step_size_bias: float32 [32], P('tp'), may hold values from -1 to 1
- head_decay_logarithm: float32 [32], P('tp'), may hold values from -14 to -3
- value_filter_taps: bfloat16 [4, 2048], P(None, 'tp'), may hold values from -3 to 3
- write_filter_taps: bfloat16 [4, 256], P(None, 'tp'), may hold values from -3 to 3
- read_filter_taps: bfloat16 [4, 256], P(None, 'tp'), may hold values from -3 to 3
- gated_group_norm_gain: float32 [2048], P('tp'), may hold values from 0.1 to 1.9
- mixer_output_weight: bfloat16 [2048, 2048], P('tp'), may hold values from -0.125 to 0.125
- residual: bfloat16 [24576, 2048], P('sp'), may hold values from -6 to 6
- feedforward_norm_gain: float32 [2048], replicated, may hold values from 0.1 to 1.9
- feedforward_gate_weight: bfloat16 [2048, 5632], P('sp', 'tp'), may hold values from -0.125 to 0.125
- feedforward_value_weight: bfloat16 [2048, 5632], P('sp', 'tp'), may hold values from -0.125 to 0.125
- gate_filter_taps: bfloat16 [3, 5632], P(None, 'tp'), may hold values from -3.5 to 3.5
- single_value_filter_taps: bfloat16 [3, 5632], P(None, 'tp'), may hold values from -3.5 to 3.5
- feedforward_down_weight: bfloat16 [5632, 2048], P('tp', 'sp'), may hold values from -0.078125 to 0.078125
Outputs:
- mixed: bfloat16 [24576, 2048], P(('sp', 'tp'))
All inputs are finite; a program needn't handle non-finite values.
Results may differ from a plain program's by a relative error of at most 0.012.
Values may be sent and summed in bfloat16 or wider, within the bound.
A program may use at most 192 MiB of HBM per device.

v0:
```python
import jax
import jax.numpy as jnp
from jax import lax
from jax.sharding import Mesh
from jax.sharding import PartitionSpec as P

HEAD = 64
STATE = 64
BLOCK = 128
SP = ("sp_0", "sp_1", "sp_2")
SP_TP = ("sp_0", "sp_1", "sp_2", "tp")


epsilon = 1e-06


def from_behind(value, axis, by):
    length = lax.axis_size(axis)
    pairs = [(i, i + by) for i in range(length) if 0 <= i + by < length]
    return lax.ppermute(value, axis, pairs)


def nothing_yet(value, identity):
    return jax.tree.map(
        lambda part, zero: jnp.zeros_like(part) + jnp.asarray(zero, part.dtype), value, identity
    )


def entering_2(value, axes, combine, identity):
    before = start = nothing_yet(value, identity)
    running = value
    for axis in reversed(axes):
        length, here = (lax.axis_size(axis), lax.axis_index(axis))
        pieces = jax.tree.map(lambda part: lax.all_gather(part, axis), running)
        inside, running = (start, start)
        for k in range(length):
            passed = k < here
            running = combine(running, jax.tree.map(lambda part: part[k], pieces))
            inside = jax.tree.map(lambda new, old: jnp.where(passed, new, old), running, inside)
        before = combine(inside, before)
    return before


def in_order(parts, dim):
    lengths = list(parts.shape[1:])
    lengths[dim] *= parts.shape[0]
    return jnp.moveaxis(parts, 0, dim).reshape(lengths)


def sent_to_all(value, axis):
    length = lax.axis_size(axis)
    return lax.all_to_all(
        jnp.broadcast_to(value[None], (length, *value.shape)), axis, 0, 0, tiled=True
    )


def gather_directly(value, axis, dim):
    return in_order(sent_to_all(value, axis), dim)


def in_one_piece(arrays, axis, dim, along):
    both = jnp.concatenate(arrays, axis=along)
    result, at, gathered = (lax.all_gather(both, axis, axis=dim, tiled=True), 0, [])
    for a in arrays:
        gathered.append(lax.slice_in_dim(result, at, at + a.shape[along], axis=along))
        at += a.shape[along]
    return tuple(gathered)


def split_up(value, dim, length):
    before, after = (value.shape[:dim], value.shape[dim + 1 :])
    return jnp.moveaxis(value.reshape(*before, length, -1, *after), dim, 0)


def sent_and_summed(value, axis, dim):
    length = lax.axis_size(axis)
    parts = lax.all_to_all(split_up(value, dim, length), axis, 0, 0, tiled=True)
    return jnp.sum(parts.astype(jnp.float32), axis=0)


def causal_taps(current, previous, kernel):
    tap_count = kernel.shape[0]
    length = current.shape[0]
    padded = jnp.concatenate([previous, current], 0).astype(jnp.float32)
    result = jnp.zeros((length, current.shape[1]), jnp.float32)
    for offset in range(tap_count):
        result = result + kernel[offset].astype(jnp.float32) * padded[offset : offset + length]
    return result


def channel_norm(stream, gain):
    floats = stream.astype(jnp.float32)
    scaled = floats * lax.rsqrt(jnp.mean(floats * floats, axis=-1, keepdims=True) + epsilon)
    return (scaled * gain).astype(jnp.bfloat16)


def on_device(
    mixer_value_projection,
    write_vectors_projected,
    read_vectors_projected,
    output_gate_projected,
    step_size_scores,
    position_decay_extra,
    step_size_bias,
    head_decay_logarithm,
    value_filter_taps,
    write_filter_taps,
    read_filter_taps,
    gated_group_norm_gain,
    mixer_output_weight,
    residual,
    feedforward_norm_gain,
    feedforward_gate_weight,
    feedforward_value_weight,
    gate_filter_taps,
    single_value_filter_taps,
    feedforward_down_weight,
):
    row_count = mixer_value_projection.shape[0]
    head_count = step_size_scores.shape[1]
    group_count = write_vectors_projected.shape[1] // STATE
    per_group = head_count // group_count
    mix_rim = value_filter_taps.shape[0] - 1
    rim_values, rim_write, rim_read = from_behind(
        (
            mixer_value_projection[row_count - mix_rim :],
            write_vectors_projected[row_count - mix_rim :],
            read_vectors_projected[row_count - mix_rim :],
        ),
        SP,
        1,
    )
    x_conv = jax.nn.silu(causal_taps(mixer_value_projection, rim_values, value_filter_taps)).astype(
        jnp.bfloat16
    )
    write_conv = jax.nn.silu(
        causal_taps(write_vectors_projected, rim_write, write_filter_taps)
    ).astype(jnp.bfloat16)
    read_conv = jax.nn.silu(causal_taps(read_vectors_projected, rim_read, read_filter_taps)).astype(
        jnp.bfloat16
    )
    step_size_head = jax.nn.softplus(step_size_scores + step_size_bias)
    logarithm_decay_rate = -step_size_head * jnp.exp(head_decay_logarithm) + position_decay_extra
    scaled = (
        x_conv.astype(jnp.float32).reshape(row_count, head_count, HEAD) * step_size_head[:, :, None]
    ).astype(jnp.bfloat16)
    block_count = row_count // BLOCK
    value_blocks = scaled.reshape(block_count, BLOCK, group_count, per_group, HEAD)
    write_blocks = write_conv.reshape(block_count, BLOCK, group_count, STATE)
    read_blocks = read_conv.reshape(block_count, BLOCK, group_count, STATE)
    running = jnp.cumsum(logarithm_decay_rate.reshape(block_count, BLOCK, head_count), axis=1)
    by_head = jnp.moveaxis(running, 1, 2)
    spread = by_head[..., :, None] - by_head[..., None, :]
    causal = jnp.tril(jnp.ones((BLOCK, BLOCK), dtype=jnp.bool_))
    decays = jnp.exp(jnp.where(causal, spread, -jnp.inf)).reshape(
        block_count, group_count, per_group, BLOCK, BLOCK
    )
    scores = jnp.einsum(
        "blgn,bsgn->bgls", read_blocks, write_blocks, preferred_element_type=jnp.float32
    )
    weights = (scores[:, :, None] * decays).astype(jnp.bfloat16)
    inside = jnp.einsum(
        "bgrls,bsgrp->blgrp", weights, value_blocks, preferred_element_type=jnp.float32
    )
    tails = jnp.moveaxis(jnp.exp(by_head[..., -1:] - by_head), 2, 1).reshape(
        block_count, BLOCK, group_count, per_group
    )
    tailed = (value_blocks.astype(jnp.float32) * tails[..., None]).astype(jnp.bfloat16)
    fresh = jnp.einsum(
        "bsgn,bsgrp->bgrnp", write_blocks, tailed, preferred_element_type=jnp.float32
    )
    block_logs = by_head[..., -1].reshape(block_count, group_count, per_group)

    def carry_step(carried, inputs):
        piece, block_log = inputs
        return (carried * jnp.exp(block_log)[..., None, None] + piece, carried)

    empty_state = jnp.zeros((group_count, per_group, STATE, HEAD), jnp.float32)
    local_end, local_before = lax.scan(carry_step, empty_state, (fresh, block_logs))
    device_log = jnp.sum(block_logs, axis=0)

    def combine(earlier, later):
        return (earlier[0] * later[0], earlier[1] * later[0][..., None, None] + later[1])

    identity = (jnp.ones((group_count, per_group), jnp.float32), empty_state)
    incoming = entering_2((jnp.exp(device_log), local_end), SP, combine, identity)[1]
    before_block = jnp.cumsum(block_logs, axis=0) - block_logs
    entering_state = local_before + incoming[None] * jnp.exp(before_block)[..., None, None]
    entering = jnp.einsum(
        "blgn,bgrnp->blgrp",
        read_blocks.astype(jnp.float32),
        entering_state,
        precision=lax.Precision.HIGHEST,
    )
    entering = (
        entering * jnp.exp(running).reshape(block_count, BLOCK, group_count, per_group)[..., None]
    )
    mixer = (inside + entering).reshape(row_count, head_count * HEAD)
    gated = (mixer * jax.nn.silu(output_gate_projected.astype(jnp.float32))).reshape(
        row_count, group_count, -1
    )
    gated = gated * lax.rsqrt(jnp.mean(gated * gated, axis=-1, keepdims=True) + epsilon)
    normed = (gated.reshape(row_count, -1) * gated_group_norm_gain).astype(jnp.bfloat16)
    share = row_count // lax.axis_size("tp")
    tp_index = lax.axis_index("tp")
    summed = lax.psum_scatter(
        jnp.dot(normed, mixer_output_weight, preferred_element_type=jnp.float32),
        "tp",
        scatter_dimension=0,
        tiled=True,
    )
    own_residual = lax.dynamic_slice_in_dim(residual, tp_index * share, share, 0)
    stream = (own_residual.astype(jnp.float32) + summed).astype(jnp.bfloat16)
    ffn_rows = gather_directly(channel_norm(stream, feedforward_norm_gain), "tp", 0)
    pieces = in_one_piece((feedforward_gate_weight, feedforward_value_weight), SP, 0, 1)
    gate_sum = jnp.dot(ffn_rows, pieces[0], preferred_element_type=jnp.float32)
    value_sum = jnp.dot(ffn_rows, pieces[1], preferred_element_type=jnp.float32)
    gate_rows = gate_sum.astype(jnp.bfloat16)
    value_rows = value_sum.astype(jnp.bfloat16)
    ffn_rim = gate_filter_taps.shape[0] - 1
    rim_gate, rim_value = from_behind(
        (gate_rows[row_count - ffn_rim :], value_rows[row_count - ffn_rim :]), SP, 1
    )
    hidden = (
        jax.nn.silu(causal_taps(gate_rows, rim_gate, gate_filter_taps))
        * causal_taps(value_rows, rim_value, single_value_filter_taps)
    ).astype(jnp.bfloat16)
    partial_down = jnp.dot(
        hidden,
        lax.all_gather(feedforward_down_weight, SP, axis=1, tiled=True),
        preferred_element_type=jnp.float32,
    )
    down = sent_and_summed(partial_down.astype(jnp.bfloat16), "tp", 0)
    return (stream.astype(jnp.float32) + down).astype(jnp.bfloat16)


def solution(mesh):
    torus = Mesh(mesh.devices.reshape(4, 4, 2, mesh.shape["tp"]), ("sp_0", "sp_1", "sp_2", "tp"))
    in_specs = (
        P(SP, "tp"),
        P(SP, "tp"),
        P(SP, "tp"),
        P(SP, "tp"),
        P(SP, "tp"),
        P(SP, "tp"),
        P("tp"),
        P("tp"),
        P(None, "tp"),
        P(None, "tp"),
        P(None, "tp"),
        P("tp"),
        P("tp", None),
        P(SP, None),
        P(),
        P(SP, "tp"),
        P(SP, "tp"),
        P(None, "tp"),
        P(None, "tp"),
        P("tp", SP),
    )
    out_specs = P(SP_TP, None)
    return jax.shard_map(
        on_device, mesh=torus, in_specs=in_specs, out_specs=out_specs, check_vma=False
    )
```

profile of v0, /device:TPU:1, one launch (start us, length us, event | category | flops | bytes accessed | tf_op | source)
XLA Modules:
  0.0 345.3 jit_solution(731696417473603664)
XLA Ops:
  9.0 4.6 %collective-permute-start = (bf16[3,512]{0,1:T(8,128)(2,1)}, bf16[3,512]{0,1:T(8,128)(2,1)}, u32[]{:S(2)}, u32[]{:S(2)}) collective-permute-start(bf16[3,512]{0,1:T(8,128)(2,1)} %copy.47), channel_id=1, source_target_pairs={{0,4},{4,8},{8,12},{12,16},{16,20},{20,24},{24,28},{28,32},{32,36}... | collective-permute-start | bytes 9224 | tf_op jit(solution)/shard_map/ppermute | solution.py:20
  13.6 1.4 slice.212
  15.0 1.9 collective-permute-start.2
  16.9 1.4 slice.203
  18.3 3.6 %collective-permute-start.1 = (bf16[3,64]{0,1:T(8,128)(2,1)}, bf16[3,64]{0,1:T(8,128)(2,1)}, u32[]{:S(2)}, u32[]{:S(2)}) collective-permute-start(bf16[3,64]{0,1:T(8,128)(2,1)} %slice.203), channel_id=1, source_target_pairs={{0,4},{4,8},{8,12},{12,16},{16,20},{20,24},{24,28},{28,32},{32,36}... | collective-permute-start | bytes 1160 | tf_op jit(solution)/shard_map/ppermute | solution.py:20
  21.9 1.4 copy.48
  24.1 1.5 fusion.68
  26.4 1.4 reduce_window_sum.22
  27.8 1.2 slice_reduce_fusion
  29.0 1.0 fusion.75
  31.4 1.2 dynamic-slice
  34.0 2.5 all-reduce
  36.4 1.3 dynamic-slice.1
  38.6 8.7 %all-reduce.1 = f32[32]{0:T(128)S(1)} all-reduce(f32[32]{0:T(128)S(1)} %fusion.73), channel_id=4, replica_groups=mesh['sp_0'=4,'sp_1'=4,'sp_2'=2,'tp'=4] {'sp_1'}, use_global_device_ids=true, to_apply=%add.1 | all-reduce | flops 32 | bytes 256
  50.1 7.2 %all_gather.34 = f32[4,1,8]{2,1,0:T(1,128)S(1)} all-gather(f32[1,1,8]{2,1,0:T(1,128)S(1)} %get-tuple-element.113), channel_id=1, replica_groups=mesh['sp_0'=4,'sp_1'=4,'sp_2'=2,'tp'=4] {'sp_0'}, dimensions={0}, use_global_device_ids=true | all-gather | bytes 160 | tf_op jit(solution)/shard_map/all_gather | solution.py:34
  58.7 1.2 copy.56
  60.7 1.7 copy.62
  62.4 2.3 copy.64
  66.6 1.6 fusion.61
  69.4 1.3 maximum_convert_fusion.2
  70.8 3.4 fusion.48
  74.1 2.7 reshape.357
  76.8 2.9 multiply_convert_fusion.1
  79.7 1.5 convolution_bitcast_fusion
  81.2 15.6 %while.13 = (s32[]{:T(128)}, f32[1,8,64,64]{3,2,1,0:T(8,128)S(1)}, f32[6,1,8,64,64]{4,3,2,1,0:T(8,128)}, f32[6,1,8]{2,1,0:T(1,128)}, f32[6,1,8,64,64]{3,4,2,0,1:T(8,128)}, /*index=5*/s32[]{:T(128)}, s32[]{:T(128)}) while((s32[]{:T(128)}, f32[1,8,64,64]{3,2,1,0:T(8,128)S(1)}, f32[6,1,8,64,64]{4,3,2,1,0:T(8,128)}, ...), condition=%wide.region_2.3_spmd.clone, body=%wide.region_1.2_spmd.clone.sunk | while | flops 131075 | bytes 1311424 | solution.py:179
  81.9 1.0 constant_dynamic-slice_fusion.3
  89.8 1.0 constant_dynamic-slice_fusion.3
  95.0 1.0 constant_dynamic-slice_fusion.3
  96.9 6.0 %all-gather.1 = f32[2,8,64,64]{3,2,1,0:T(8,128)S(1)} all-gather(f32[1,8,64,64]{3,2,1,0:T(8,128)S(1)} %get-tuple-element.34), channel_id=3, replica_groups=mesh['sp_0'=4,'sp_1'=4,'sp_2'=2,'tp'=4] {'sp_2'}, dimensions={0}, use_global_device_ids=true | all-gather | bytes 393216 | tf_op jit(solution)/shard_map/all_gather | solution.py:34
  103.1 12.3 %all_gather.37 = f32[4,1,8,64,64]{4,3,2,1,0:T(8,128)S(1)} all-gather(f32[1,1,8,64,64]{4,3,2,1,0:T(8,128)S(1)} %fusion.53), channel_id=1, replica_groups=mesh['sp_0'=4,'sp_1'=4,'sp_2'=2,'tp'=4] {'sp_1'}, dimensions={0}, use_global_device_ids=true | all-gather | bytes 655360 | tf_op jit(solution)/shard_map/all_gather | solution.py:34
  115.6 13.0 %all_gather.38 = f32[4,1,8,64,64]{4,3,2,1,0:T(8,128)S(1)} all-gather(f32[1,1,8,64,64]{4,3,2,1,0:T(8,128)S(1)} %slice_add_fusion.4), channel_id=1, replica_groups=mesh['sp_0'=4,'sp_1'=4,'sp_2'=2,'tp'=4] {'sp_0'}, dimensions={0}, use_global_device_ids=true | all-gather | bytes 655360 | tf_op jit(solution)/shard_map/all_gather | solution.py:34
  129.1 1.5 fusion.32
  130.6 1.3 fusion.31
  133.6 4.8 %fusion.41 = f32[768,2048]{1,0:T(8,128)} fusion(bf16[512,2048]{1,0:T(8,128)(2,1)S(1)} %copy-done, f32[512]{0:T(512)S(1)} %copy-done.33, f32[768]{0:T(1024)S(1)} %add_rsqrt_fusion, bf16[768,512]{0,1:T(8,128)(2,1)S(1)} %copy-done.2, f32[64,8,6,128]{3,2,1,0:T(8,128)S(1)} %bitcast.139), kind=kOutput, calls=%fused_computation.69 | convolution fusion | flops 1614151680 | bytes 10753024 | tf_op jit(solution)/shard_map/dot_general | solution.py:207
  140.8 64.3 %reduce-scatter.2.cloned.1.call-done = f32[192,2048]{1,0:T(8,128)} async-done(((f32[768,2048]{1,0:T(8,128)}), f32[192,2048]{1,0:T(8,128)}) %reduce-scatter.2.cloned.1.call-update) | async-done | bytes 1572880 | tf_op jit(solution)/shard_map/reduce_scatter | solution.py:206
  205.1 1.9 fusion.23
  207.3 2.0 broadcast_in_dim.34
  209.3 4.8 %all-to-all-start = ((bf16[4,192,2048]{2,1,0:T(8,128)(2,1)}), bf16[4,192,2048]{2,1,0:T(8,128)(2,1)}, u32[]{:S(2)}, u32[]{:S(2)}) async-start(bf16[4,192,2048]{2,1,0:T(8,128)(2,1)} %broadcast_in_dim.34), calls=%async_computation.1 | async-start | bytes 6291456 | tf_op jit(solution)/shard_map/all_to_all | solution.py:52
  214.3 36.9 %all-to-all-done = bf16[4,192,2048]{2,1,0:T(8,128)(2,1)} async-done(((bf16[4,192,2048]{2,1,0:T(8,128)(2,1)}), bf16[4,192,2048]{2,1,0:T(8,128)(2,1)}, u32[]{:S(2)}, u32[]{:S(2)}) %all-to-all-start) | async-done | bytes 3145760 | tf_op jit(solution)/shard_map/all_to_all | solution.py:52
  251.1 8.5 %fusion.12 = bf16[768,1408]{1,0:T(8,128)(2,1)S(1)} fusion(bf16[768,2048]{1,0:T(8,128)(2,1)} %bitcast.35, bf16[2048,2816]{1,0:T(8,128)(2,1)} %all-gather.6.cloned.1.call-done), kind=kOutput, calls=%fused_computation.23 | convolution fusion | flops 4430266368 | bytes 11075584 | tf_op jit(solution)/shard_map/dot_general | solution.py:216
  259.7 4.6 %collective-permute-start.3 = (bf16[2,1408]{1,0:T(2,128)(2,1)S(1)}, bf16[2,1408]{1,0:T(2,128)(2,1)S(1)}, u32[]{:S(2)}, u32[]{:S(2)}) collective-permute-start(bf16[2,1408]{1,0:T(2,128)(2,1)S(1)} %slice.293), channel_id=1, source_target_pairs={{0,4},{4,8},{8,12},{12,16},{16,20},{20,24},{24,28},{28,32},{32,36}... | collective-permute-start | bytes 16904 | tf_op jit(solution)/shard_map/ppermute | solution.py:20
  264.2 6.7 %fusion.15 = bf16[768,1408]{1,0:T(8,128)(2,1)S(1)} fusion(bf16[768,2048]{1,0:T(8,128)(2,1)} %bitcast.35, bf16[2048,2816]{1,0:T(8,128)(2,1)S(1)} %copy-done.32), kind=kOutput, calls=%fused_computation.24 | convolution fusion | flops 4430266368 | bytes 11075584 | tf_op jit(solution)/shard_map/dot_general | solution.py:217
  271.0 2.1 collective-permute-start.4
  273.1 2.5 maximum_convert_fusion
  275.6 2.4 maximum_convert_fusion.1
  278.1 17.3 %convolution_convert_fusion = bf16[768,2048]{1,0:T(8,128)(2,1)} fusion(bf16[1408,2048]{0,1:T(8,128)(2,1)} %all-gather.8.cloned.1.call-done, f32[770,1408]{1,0:T(8,128)} %maximum_convert_fusion.1, f32[770,1408]{1,0:T(8,128)} %maximum_convert_fusion, f32[1408]{0:T(1024)S(1)} %get-tuple-element.72, f32[1408]{0:T(1024)S(1)} %get-tuple-element.73, ...), kind=kOutput, calls=%fused_computation.25 | convolution fusion | flops 4448059392 | bytes 34898944 | tf_op jit(solution)/shard_map/dot_general | solution.py:228
  295.4 40.8 %all_to_all.10 = bf16[4,192,2048]{2,1,0:T(8,128)(2,1)S(1)} all-to-all(bf16[4,192,2048]{2,1,0:T(8,128)(2,1)} %bitcast.142), channel_id=1, replica_groups=mesh['sp_0'=4,'sp_1'=4,'sp_2'=2,'tp'=4] {'tp'}, dimensions={0} | all-to-all | bytes 6291456 | tf_op jit(solution)/shard_map/all_to_all | solution.py:77
  336.8 1.1 fusion.26
  (151 shorter events, 31.9 us)
Async XLA Ops:
  7.4 126.2 %copy-start = (bf16[512,2048]{1,0:T(8,128)(2,1)S(1)}, bf16[512,2048]{1,0:T(8,128)(2,1)}, u32[]{:S(2)}) copy-start(bf16[512,2048]{1,0:T(8,128)(2,1)} %param.34) | copy-start | bytes 6291460
  7.4 197.7 %reduce-scatter.2.cloned.1.call-start = ((), (), s32[]{:S(2)}) async-start(), calls=%async_computation.3 | async-start | bytes 7864320 | tf_op jit(solution)/shard_map/reduce_scatter | solution.py:206
  9.0 60.4 %collective-permute-start = (bf16[3,512]{0,1:T(8,128)(2,1)}, bf16[3,512]{0,1:T(8,128)(2,1)}, u32[]{:S(2)}, u32[]{:S(2)}) collective-permute-start(bf16[3,512]{0,1:T(8,128)(2,1)} %copy.47), channel_id=1, source_target_pairs={{0,4},{4,8},{8,12},{12,16},{16,20},{20,24},{24,28},{28,32},{32,36}... | collective-permute-start | bytes 9224 | tf_op jit(solution)/shard_map/ppermute | solution.py:20
  15.0 49.7 %collective-permute-start.2 = (bf16[3,64]{0,1:T(8,128)(2,1)}, bf16[3,64]{0,1:T(8,128)(2,1)}, u32[]{:S(2)}, u32[]{:S(2)}) collective-permute-start(bf16[3,64]{0,1:T(8,128)(2,1)} %slice.212), channel_id=1, source_target_pairs={{0,4},{4,8},{8,12},{12,16},{16,20},{20,24},{24,28},{28,32},{32,36}... | collective-permute-start | bytes 1160 | tf_op jit(solution)/shard_map/ppermute | solution.py:20
  18.3 47.5 %collective-permute-start.1 = (bf16[3,64]{0,1:T(8,128)(2,1)}, bf16[3,64]{0,1:T(8,128)(2,1)}, u32[]{:S(2)}, u32[]{:S(2)}) collective-permute-start(bf16[3,64]{0,1:T(8,128)(2,1)} %slice.203), channel_id=1, source_target_pairs={{0,4},{4,8},{8,12},{12,16},{16,20},{20,24},{24,28},{28,32},{32,36}... | collective-permute-start | bytes 1160 | tf_op jit(solution)/shard_map/ppermute | solution.py:20
  21.9 25.4 %copy-start.15 = (bf16[4,512]{1,0:T(4,128)(2,1)S(1)}, bf16[4,512]{1,0:T(4,128)(2,1)}, u32[]{:S(2)}) copy-start(bf16[4,512]{1,0:T(4,128)(2,1)} %param.30) | copy-start | bytes 12292
  30.7 33.9 %copy-start.8 = (bf16[768,64]{0,1:T(8,128)(2,1)S(1)}, bf16[768,64]{0,1:T(8,128)(2,1)}, u32[]{:S(2)}) copy-start(bf16[768,64]{0,1:T(8,128)(2,1)} %param.23) | copy-start | bytes 294916
  30.7 35.0 %copy-start.9 = (bf16[768,64]{0,1:T(8,128)(2,1)S(1)}, bf16[768,64]{0,1:T(8,128)(2,1)}, u32[]{:S(2)}) copy-start(bf16[768,64]{0,1:T(8,128)(2,1)} %param.24) | copy-start | bytes 294916
  68.2 2.5 copy-start.17
  68.2 2.6 copy-start.18
  68.2 2.6 copy-start.19
  81.2 21.7 %copy-start.24 = (f32[8]{0:T(128)S(1)}, f32[8]{0:T(128)}, u32[]{:S(2)}) copy-start(f32[8]{0:T(128)} %get-tuple-element.114) | copy-start | bytes 100
  81.2 21.7 %copy-start.25 = (f32[8]{0:T(128)S(1)}, f32[8]{0:T(128)}, u32[]{:S(2)}) copy-start(f32[8]{0:T(128)} %get-tuple-element.115) | copy-start | bytes 100
  96.8 18.6 %copy-start.20 = (f32[8]{0:T(128)S(1)}, f32[8]{0:T(128)}, u32[]{:S(2)}) copy-start(f32[8]{0:T(128)} %get-tuple-element.116) | copy-start | bytes 100
  96.9 18.5 %copy-start.21 = (f32[8]{0:T(128)S(1)}, f32[8]{0:T(128)}, u32[]{:S(2)}) copy-start(f32[8]{0:T(128)} %get-tuple-element.117) | copy-start | bytes 100
  96.9 18.5 %copy-start.22 = (f32[8]{0:T(128)S(1)}, f32[8]{0:T(128)}, u32[]{:S(2)}) copy-start(f32[8]{0:T(128)} %get-tuple-element.118) | copy-start | bytes 100
  96.9 18.5 %copy-start.23 = (f32[8]{0:T(128)S(1)}, f32[8]{0:T(128)}, u32[]{:S(2)}) copy-start(f32[8]{0:T(128)} %get-tuple-element.119) | copy-start | bytes 100
  103.0 25.5 %copy-start.26 = (f32[8]{0:T(128)S(1)}, f32[8]{0:T(128)}, u32[]{:S(2)}) copy-start(f32[8]{0:T(128)} %get-tuple-element.86) | copy-start | bytes 100
  103.0 25.5 %copy-start.27 = (f32[8]{0:T(128)S(1)}, f32[8]{0:T(128)}, u32[]{:S(2)}) copy-start(f32[8]{0:T(128)} %get-tuple-element.87) | copy-start | bytes 100
  103.0 25.5 %copy-start.28 = (f32[8]{0:T(128)S(1)}, f32[8]{0:T(128)}, u32[]{:S(2)}) copy-start(f32[8]{0:T(128)} %get-tuple-element.101) | copy-start | bytes 100
  103.0 25.5 %copy-start.29 = (f32[8]{0:T(128)S(1)}, f32[8]{0:T(128)}, u32[]{:S(2)}) copy-start(f32[8]{0:T(128)} %get-tuple-element.102) | copy-start | bytes 100
  103.0 25.5 %copy-start.30 = (f32[8]{0:T(128)S(1)}, f32[8]{0:T(128)}, u32[]{:S(2)}) copy-start(f32[8]{0:T(128)} %get-tuple-element.103) | copy-start | bytes 100
  103.1 25.5 %copy-start.31 = (f32[8]{0:T(128)S(1)}, f32[8]{0:T(128)}, u32[]{:S(2)}) copy-start(f32[8]{0:T(128)} %get-tuple-element.104) | copy-start | bytes 100
  115.6 13.5 %copy-start.3 = (f32[6,1,8,64,64]{4,3,2,1,0:T(8,128)S(1)}, f32[6,1,8,64,64]{4,3,2,1,0:T(8,128)}, u32[]{:S(2)}) copy-start(f32[6,1,8,64,64]{4,3,2,1,0:T(8,128)} %get-tuple-element.33) | copy-start | bytes 2359300
  115.6 13.5 %copy-start.5 = (bf16[6,128,64]{1,0,2:T(8,128)(2,1)S(1)}, bf16[6,128,64]{1,0,2:T(8,128)(2,1)}, u32[]{:S(2)}) copy-start(bf16[6,128,64]{1,0,2:T(8,128)(2,1)} %reshape.345) | copy-start | bytes 294916
  129.0 1.6 copy-start.4
  129.0 1.6 copy-start.12
  129.0 1.6 copy-start.13
  129.0 1.6 copy-start.14
  129.0 1.6 copy-start.34
  131.9 1.1 copy-start.2
  132.8 0.8 copy-start.33
  138.4 0.9 copy-start.6
  138.4 1.0 copy-start.7
  138.4 68.6 %copy-start.16 = (f32[2048]{0:T(1024)S(1)}, f32[2048]{0:T(1024)}, u32[]{:S(2)}) copy-start(f32[2048]{0:T(1024)} %param.36) | copy-start | bytes 24580
  138.4 112.7 %all-gather.6.cloned.1.call-start = ((), (), s32[]{:S(2)}) async-start(), calls=%async_computation.4 | async-start | bytes 11894784 | tf_op jit(solution)/shard_map/all_gather | solution.py:63
  140.2 137.9 %all-gather.8.cloned.1.call-start = ((), (), s32[]{:S(2)}) async-start(), calls=%async_computation.5 | async-start | bytes 5947392 | tf_op jit(solution)/shard_map/all_gather | solution.py:230
  209.3 4.8 %copy-start.10 = (bf16[3,1408]{1,0:T(4,128)(2,1)S(1)}, bf16[3,1408]{1,0:T(4,128)(2,1)}, u32[]{:S(2)}) copy-start(bf16[3,1408]{1,0:T(4,128)(2,1)} %param.40) | copy-start | bytes 25348
  209.3 4.8 %copy-start.11 = (bf16[3,1408]{1,0:T(4,128)(2,1)S(1)}, bf16[3,1408]{1,0:T(4,128)(2,1)}, u32[]{:S(2)}) copy-start(bf16[3,1408]{1,0:T(4,128)(2,1)} %param.39) | copy-start | bytes 25348
  209.3 41.8 %all-to-all-start = ((bf16[4,192,2048]{2,1,0:T(8,128)(2,1)}), bf16[4,192,2048]{2,1,0:T(8,128)(2,1)}, u32[]{:S(2)}, u32[]{:S(2)}) async-start(bf16[4,192,2048]{2,1,0:T(8,128)(2,1)} %broadcast_in_dim.34), calls=%async_computation.1 | async-start | bytes 6291456 | tf_op jit(solution)/shard_map/all_to_all | solution.py:52
  251.1 13.1 %copy-start.32 = (bf16[2048,2816]{1,0:T(8,128)(2,1)S(1)}, bf16[2048,2816]{1,0:T(8,128)(2,1)}, u32[]{:S(2)}) copy-start(bf16[2048,2816]{1,0:T(8,128)(2,1)} %all-gather.6.cloned.1.call-done) | copy-start | bytes 34603012
  259.7 13.4 %collective-permute-start.3 = (bf16[2,1408]{1,0:T(2,128)(2,1)S(1)}, bf16[2,1408]{1,0:T(2,128)(2,1)S(1)}, u32[]{:S(2)}, u32[]{:S(2)}) collective-permute-start(bf16[2,1408]{1,0:T(2,128)(2,1)S(1)} %slice.293), channel_id=1, source_target_pairs={{0,4},{4,8},{8,12},{12,16},{16,20},{20,24},{24,28},{28,32},{32,36}... | collective-permute-start | bytes 16904 | tf_op jit(solution)/shard_map/ppermute | solution.py:20
  271.0 4.7 %collective-permute-start.4 = (bf16[2,1408]{1,0:T(2,128)(2,1)S(1)}, bf16[2,1408]{1,0:T(2,128)(2,1)S(1)}, u32[]{:S(2)}, u32[]{:S(2)}) collective-permute-start(bf16[2,1408]{1,0:T(2,128)(2,1)S(1)} %slice.298), channel_id=1, source_target_pairs={{0,4},{4,8},{8,12},{12,16},{16,20},{20,24},{24,28},{28,32},{32,36}... | collective-permute-start | bytes 16904 | tf_op jit(solution)/shard_map/ppermute | solution.py:20
  336.2 1.7 copy-start.1
Sparse Core Ops, SparseCore 0:
  138.5 66.5 reduce-scatter.1
Sparse Core Ops, SparseCore 1:
  141.2 63.3 all-gather.5
  206.6 47.6 all-gather.7
where the time goes:
time: 347 us; the launch traced here: 345 us
  waiting for transfers between devices  102 us (29%)
  blocking collectives  90.5 us (26%)
  matrix products  43.1 us (12%)
  local copies, waits for them, and re-layouts  36.4 us (10%)
  other arithmetic  34.8 us (10%)
  starting transfers between devices  21.6 us (6%)
  between operations  16.8 us (5%)
    reduce_scatter x1, waiting for transfers between devices, on_device(): lax.psum_scatter(jnp.dot(normed, mixer_output_weight, preferred_element_t...  64.3 us
    all_to_all x1, blocking collectives, sent_and_summed(): parts = lax.all_to_all(split_up(value, dim, length), axis, 0, 0, tiled=True)  40.8 us
    all_gather x4, blocking collectives, entering_2(): pieces = jax.tree.map(lambda part: lax.all_gather(part, axis), running)  38.5 us
    all_to_all x1, waiting for transfers between devices, sent_to_all(): lax.all_to_all(jnp.broadcast_to(value[None], (length, *value.shape)), axi...  36.9 us
    dot_general x1, matrix products, on_device(): jnp.dot(hidden, lax.all_gather(feedforward_down_weight, SP, axis=1, tiled...  17.3 us
    ppermute x5, starting transfers between devices, from_behind(): return lax.ppermute(value, axis, pairs)  16.8 us
    unnamed x2, blocking collectives  11.2 us
    dot_general x1, matrix products, on_device(): gate_sum = jnp.dot(ffn_rows, pieces[0], preferred_element_type=jnp.float32)  8.51 us
  transfers between devices with their start and end apart: 9, of which 2 were waited for; matrix products, arithmetic and copies ran while one was open for 16% of the time, Pallas kernels for 0%

commit v1 on v0

v1 whole, which is shorter than its diff:
```python
import functools

import jax
import jax.numpy as jnp
from jax import lax
from jax.experimental import pallas as pl
from jax.experimental.pallas import tpu as pltpu
from jax.sharding import Mesh
from jax.sharding import PartitionSpec as P

SP = ("sp_0", "sp_1", "sp_2")
SP_TP = ("sp_0", "sp_1", "sp_2", "tp")
MESH = pl.DeviceIdType.MESH
EPS = 1e-06
F32 = jnp.float32
BF16 = jnp.bfloat16
HI = lax.Precision.HIGHEST

ROWS = 768
BLOCK = 128
BLOCKS = 6
HEADS = 8
INNER = 512
WIDTH = 2048
HIDDEN = 1408
SHARE = 192


def silu(v):
    return v / (1.0 + jnp.exp(-v))


def dot(a, b):
    return jnp.dot(a, b, preferred_element_type=F32)


def kernel(
    xv, wrt, rdt, og, sct, ext, bias, hlog, vtap, bctap, ggain, wout, res, fgain, gw, vw, gtap, vtap2, dwt,
    out,
    xs, bct, ogs, st_s, cum_s, bt_s, c_s, sc_s, ecx_s, ins_s, lb_s, pre_s, stv, plog,
    m1, r1, r2, r3, inc,
    ng, stream, fin, wof, gvd, hid, sbuf, ra, rb, rl, rr, own,
    lsem, hsend, hrecv, xsend, xrecv, ssend, srecv, wsend, wrecv, asend, arecv, qsend, qrecv,
):
    z = lax.axis_index("sp_0")
    y = lax.axis_index("sp_1")
    c = lax.axis_index("sp_2")
    x = lax.axis_index("tp")
    sp = z * 8 + y * 2 + c

    def at_sp(s):
        return ((s // 8) % 4, (s // 2) % 4, s % 2, x)

    nxt = at_sp(sp + 1)
    prv = at_sp(sp + 31)
    partner = (z, y, 1 - c, x)

    def dev_x(d):
        return (z, y, c, (x + d + 4) % 4)

    def dev_y(d):
        return (z, (y + d) % 4, c, x)

    def dev_z(d):
        return ((z + d) % 4, y, c, x)

    def dev1(d):
        return ((z + 4 + d * c) % 4, (y + 4 + d * (1 - c)) % 4, c, x)

    def dev2(d):
        return ((z + 4 + d * (1 - c)) % 4, (y + 4 + d * c) % 4, c, x)

    ca = c * z + (1 - c) * y
    cb = c * y + (1 - c) * z

    def item(da, db):
        return ((ca + 4 + da) % 4) * (2 + 6 * c) + ((cb + 4 + db) % 4) * (8 - 6 * c) + c

    def remote(src, dst, ss, rs, dev):
        return pltpu.make_async_remote_copy(
            src_ref=src, dst_ref=dst, send_sem=ss, recv_sem=rs, device_id=dev, device_id_type=MESH
        )

    loads = [
        pltpu.make_async_copy(xv, xs.at[pl.ds(16, ROWS)], lsem.at[0]),
        pltpu.make_async_copy(wrt, bct.at[pl.ds(0, 64), pl.ds(128, ROWS)], lsem.at[1]),
        pltpu.make_async_copy(rdt, bct.at[pl.ds(64, 64), pl.ds(128, ROWS)], lsem.at[2]),
        pltpu.make_async_copy(gw, gvd.at[sp, 0], lsem.at[3]),
        pltpu.make_async_copy(vw, gvd.at[sp, 1], lsem.at[4]),
        pltpu.make_async_copy(dwt, gvd.at[sp, 2], lsem.at[5]),
        pltpu.make_async_copy(og, ogs, lsem.at[6]),
        pltpu.make_async_copy(wout, wof.at[0], lsem.at[7]),
        pltpu.make_async_copy(res, stream, lsem.at[8]),
    ]
    for load in loads:
        load.start()

    barrier = pltpu.get_barrier_semaphore()
    peers = [partner, nxt, prv]
    for d in (1, 2, 3):
        peers += [dev_x(d), dev_y(d), dev_z(d)]
    for peer in peers:
        pl.semaphore_signal(barrier, inc=1, device_id=peer, device_id_type=MESH)
    pl.semaphore_wait(barrier, len(peers))

    pending = []

    def start(copy):
        copy.start()
        pending.append(copy)

    halo = [
        remote(xv.at[pl.ds(ROWS - 16, 16)], xs.at[pl.ds(0, 16)], hsend.at[0], hrecv.at[0], nxt),
        remote(wrt.at[:, pl.ds(ROWS - 128, 128)], bct.at[pl.ds(0, 64), pl.ds(0, 128)], hsend.at[1], hrecv.at[1], nxt),
        remote(rdt.at[:, pl.ds(ROWS - 128, 128)], bct.at[pl.ds(64, 64), pl.ds(0, 128)], hsend.at[2], hrecv.at[2], nxt),
    ]

    @pl.when(sp < 31)
    def _():
        for h in halo:
            h.start()

    @pl.when(sp == 0)
    def _():
        xs[pl.ds(0, 16), :] = jnp.zeros((16, INNER), BF16)
        bct[:, pl.ds(0, 128)] = jnp.zeros((128, 128), BF16)
        fin[pl.ds(0, 16), :] = jnp.zeros((16, WIDTH), BF16)

    for r in (1, 2, 3):
        start(remote(wout.at[sp], wof.at[r, sp], xsend.at[r - 1], xrecv.at[r - 1], dev_x(-r)))

    def full(batch, k):
        if batch == 0:
            return wof.at[pl.ds(1, 3), k]
        if batch == 1:
            return gvd.at[k, pl.ds(0, 2)]
        return gvd.at[k, 2]

    def half(batch, k, side):
        if batch == 0:
            return wof.at[pl.ds(1, 3), k, :, pl.ds(1024 * side, 1024)]
        if batch == 1:
            return gvd.at[k, side]
        return gvd.at[k, 2, pl.ds(32 * side, 32)]

    def send(batch, ref, sem, dev):
        start(remote(ref, ref, wsend.at[batch, sem], wrecv.at[batch, sem], dev))

    def arrive(batch, ref, sem):
        remote(ref, ref, wsend.at[batch, sem], wrecv.at[batch, sem], partner).wait_recv()

    def to_partner(batch, k):
        ref = full(batch, k)
        start(remote(ref, ref, wsend.at[batch, 20 + k // 2], wrecv.at[batch, 20 + k // 2], partner))

    order = (0, -1, 1, 2)

    def first_sends(batch):
        k = item(0, 0)
        send(batch, full(batch, k), 1, dev1(-1))
        send(batch, full(batch, k), 0, dev1(1))
        second_sends(batch, 0)

    def second_sends(batch, j):
        k = item(order[j], 0)
        send(batch, full(batch, k), 4 + 4 * j + 1, dev2(-1))
        send(batch, full(batch, k), 4 + 4 * j, dev2(1))
        to_partner(batch, k)

    def first_events(batch):
        k = item(-1, 0)
        arrive(batch, full(batch, k), 0)
        send(batch, half(batch, k, 0), 2, dev1(1))
        k2 = item(1, 0)
        arrive(batch, full(batch, k2), 1)
        send(batch, half(batch, k2, 1), 3, dev1(-1))
        second_sends(batch, 1)
        second_sends(batch, 2)

    def third_event(batch):
        k = item(2, 0)
        arrive(batch, half(batch, k, 0), 2)
        arrive(batch, half(batch, k, 1), 3)
        second_sends(batch, 3)

    def second_events(batch, j):
        base = 4 + 4 * j
        k = item(order[j], -1)
        arrive(batch, full(batch, k), base)
        send(batch, half(batch, k, 0), base + 2, dev2(1))
        to_partner(batch, k)
        k = item(order[j], 1)
        arrive(batch, full(batch, k), base + 1)
        send(batch, half(batch, k, 1), base + 3, dev2(-1))
        to_partner(batch, k)

    def last_events(batch, j):
        base = 4 + 4 * j
        k = item(order[j], 2)
        arrive(batch, half(batch, k, 0), base + 2)
        arrive(batch, half(batch, k, 1), base + 3)
        to_partner(batch, k)

    def from_partner(batch):
        for i in range(16):
            arrive(batch, full(batch, 2 * i + 1 - c), 20 + i)

    for i in (3, 4, 5):
        loads[i].wait()
    for batch in (1, 2):
        k = item(0, 0)
        send(batch, full(batch, k), 1, dev1(-1))
        send(batch, full(batch, k), 0, dev1(1))

    head = lax.broadcasted_iota(jnp.int32, (HEADS, 1), 0)
    bias_c = jnp.zeros((HEADS, 1), F32)
    rate_c = jnp.zeros((HEADS, 1), F32)
    for h in range(HEADS):
        bias_c = jnp.where(head == h, bias[h], bias_c)
        rate_c = jnp.where(head == h, hlog[h], rate_c)
    rate_c = jnp.exp(rate_c)
    v = sct[...] + bias_c
    step = jnp.maximum(v, 0.0) + jnp.log1p(jnp.exp(-jnp.abs(v)))
    logd = -step * rate_c + ext[...]
    row_i = lax.broadcasted_iota(jnp.int32, (BLOCK, BLOCK), 0)
    col_i = lax.broadcasted_iota(jnp.int32, (BLOCK, BLOCK), 1)
    upper = (row_i <= col_i).astype(F32)
    for b in range(BLOCKS):
        st_s[b] = step[:, b * BLOCK : (b + 1) * BLOCK]
        cum_s[b] = jnp.dot(
            logd[:, b * BLOCK : (b + 1) * BLOCK], upper, preferred_element_type=F32, precision=HI
        )

    def expand(value):
        spread = (
            lax.broadcasted_iota(jnp.int32, (HEADS, INNER), 1) // 64
            == lax.broadcasted_iota(jnp.int32, (HEADS, INNER), 0)
        ).astype(F32)
        return jnp.dot(value.T, spread, preferred_element_type=F32, precision=HI)

    loads[0].wait()
    loads[1].wait()
    loads[2].wait()

    @pl.when(sp > 0)
    def _():
        for h in halo:
            h.wait_recv()

    stv[...] = jnp.zeros_like(stv)
    plog[...] = jnp.zeros_like(plog)
    vt = vtap[...].astype(F32)
    bt = bctap[...].astype(F32)

    def local(b, _):
        r0 = pl.multiple_of(b * BLOCK, BLOCK)
        rows = xs[pl.ds(r0, BLOCK + 16), :].astype(F32)
        conv = vt[3:4] * rows
        for j in range(3):
            conv = conv + vt[j : j + 1] * pltpu.roll(rows, 3 - j, 0)
        xc = silu(conv[16:]).astype(BF16).astype(F32)
        lanes = bct[:, pl.ds(r0, 2 * BLOCK)].astype(F32)
        conv2 = bt[:, 3:4] * lanes
        for j in range(3):
            conv2 = conv2 + bt[:, j : j + 1] * pltpu.roll(lanes, 3 - j, 1)
        bc = silu(conv2[:, BLOCK:])
        wt = bc[:64].astype(BF16)
        rd = bc[64:].T.astype(BF16)
        bt_s[b] = wt
        c_s[b] = rd
        cumx = expand(cum_s[b])
        stepx = expand(st_s[b])
        last = cumx[BLOCK - 1 : BLOCK]
        scaled = (xc * stepx).astype(BF16)
        sc_s[pl.ds(r0, BLOCK), :] = scaled
        tailed = (scaled.astype(F32) * jnp.exp(last - cumx)).astype(BF16)
        ecx_s[pl.ds(r0, BLOCK), :] = jnp.exp(cumx)
        fresh = dot(wt, tailed)
        lb_s[b] = stv[...]
        pre_s[b] = plog[...]
        stv[...] = stv[...] * jnp.exp(last) + fresh
        plog[...] = plog[...] + last
        return 0

    def inner(b, _):
        r0 = pl.multiple_of(b * BLOCK, BLOCK)
        s = dot(c_s[b], bt_s[b])
        cum = cum_s[b]
        cumt = cum.T
        causal = (
            lax.broadcasted_iota(jnp.int32, (BLOCK, BLOCK), 0)
            >= lax.broadcasted_iota(jnp.int32, (BLOCK, BLOCK), 1)
        )
        low = lax.broadcasted_iota(jnp.int32, (BLOCK, BLOCK), 1) < 64
        for p in range(HEADS // 2):
            rhs = sc_s[pl.ds(r0, BLOCK), pl.ds(p * 128, 128)]
            parts = []
            for h in (2 * p, 2 * p + 1):
                spread = jnp.where(causal, cumt[:, h : h + 1] - cum[h : h + 1, :], -jnp.inf)
                parts.append(dot((s * jnp.exp(spread)).astype(BF16), rhs))
            ins_s[pl.ds(r0, BLOCK), pl.ds(p * 128, 128)] = jnp.where(low, parts[0], parts[1])
        return 0

    def put(ref, decay, state):
        ref[pl.ds(0, 64), :] = state.astype(BF16)
        d = jnp.broadcast_to(decay, (16, INNER))
        high = d.astype(BF16)
        ref[pl.ds(64, 16), :] = high
        ref[pl.ds(80, 16), :] = (d - high.astype(F32)).astype(BF16)

    def take(ref):
        decay = ref[pl.ds(64, 16), :].astype(F32) + ref[pl.ds(80, 16), :].astype(F32)
        return decay[0:1], ref[pl.ds(0, 64), :].astype(F32)

    def wait_pieces():
        for r in (1, 2, 3):
            remote(wout.at[sp], wof.at[r, sp], xsend.at[r - 1], xrecv.at[r - 1], dev_x(-r)).wait_recv()

    lax.fori_loop(0, 3, local, 0)
    wait_pieces()
    first_sends(0)
    lax.fori_loop(3, 6, local, 0)

    put(m1, jnp.exp(plog[...]), stv[...])
    first_events(0)
    start(remote(m1, r1, ssend.at[0], srecv.at[0], partner))
    lax.fori_loop(0, 3, inner, 0)
    remote(m1, r1, ssend.at[0], srecv.at[0], partner).wait_recv()
    d_own, s_own = jnp.exp(plog[...]), stv[...]
    d_par, s_par = take(r1)
    is_first = c == 0
    chip_d = d_own * d_par
    chip_s = jnp.where(is_first, s_own * d_par + s_par, s_par * d_own + s_own)
    put(r2.at[y], chip_d, chip_s)
    third_event(0)
    for d in (1, 2, 3):
        start(remote(r2.at[y], r2.at[y], ssend.at[d], srecv.at[d], dev_y(d)))
    lax.fori_loop(3, 6, inner, 0)
    for j in (0, 1):
        second_events(0, j)
    for d in (1, 2, 3):
        src = (y + 4 - d) % 4
        remote(r2.at[src], r2.at[src], ssend.at[d], srecv.at[d], dev_y(d)).wait_recv()
    row_d, row_s = take(r2.at[0])
    exc_d = jnp.where(y > 0, row_d, 1.0)
    exc_s = jnp.where(y > 0, row_s, 0.0)
    for i in (1, 2, 3):
        di, si = take(r2.at[i])
        row_s = row_s * di + si
        row_d = row_d * di
        exc_s = jnp.where(y > i, exc_s * di + si, exc_s)
        exc_d = jnp.where(y > i, exc_d * di, exc_d)
    put(r3.at[z], row_d, row_s)
    inc[0] = exc_s
    inc[1] = jnp.broadcast_to(exc_d, (64, INNER))
    for j in (2, 3):
        second_events(0, j)
    for d in (1, 2, 3):
        start(remote(r3.at[z], r3.at[z], ssend.at[3 + d], srecv.at[3 + d], dev_z(d)))
    for j in range(4):
        last_events(0, j)
    for d in (1, 2, 3):
        src = (z + 4 - d) % 4
        remote(r3.at[src], r3.at[src], ssend.at[3 + d], srecv.at[3 + d], dev_z(d)).wait_recv()
    acc = jnp.zeros((64, INNER), F32)
    for i in (0, 1, 2):
        di, si = take(r3.at[i])
        acc = jnp.where(z > i, acc * di + si, acc)
    acc = acc * inc[1] + inc[0]
    d_par, s_par = take(r1)
    inc[0] = jnp.where(is_first, acc, acc * d_par + s_par)

    for batch in (1, 2):
        second_sends(batch, 0)
        first_events(batch)
        third_event(batch)

    loads[6].wait()
    gain = ggain[...]

    def block_of(i):
        return (i + 4) % 6

    def rows_of(i):
        return pl.multiple_of(block_of(i) * BLOCK, BLOCK)

    def ng_full(r, i):
        return ng.at[r, pl.ds(rows_of(i), BLOCK)]

    def ng_half(r, i, side):
        return ng.at[r, pl.ds(pl.multiple_of(rows_of(i) + 64 * side, 64), 64)]

    def ag_right(i):
        return remote(ng_full(0, i), ng_full(3, i), asend.at[0, i], arecv.at[0, i], dev_x(1))

    def ag_left(i):
        return remote(ng_full(0, i), ng_full(1, i), asend.at[1, i], arecv.at[1, i], dev_x(-1))

    def ag_forward_right(i):
        return remote(ng_half(3, i, 0), ng_half(2, i, 0), asend.at[2, i], arecv.at[2, i], dev_x(1))

    def ag_forward_left(i):
        return remote(ng_half(1, i, 1), ng_half(2, i, 1), asend.at[3, i], arecv.at[3, i], dev_x(-1))

    def final(i, _):
        b = block_of(i)
        r0 = rows_of(i)
        state = lb_s[b] + inc[0] * jnp.exp(pre_s[b])
        ent = dot(c_s[b], state.astype(BF16))
        m = ins_s[pl.ds(r0, BLOCK), :] + ecx_s[pl.ds(r0, BLOCK), :] * ent
        g = m * silu(ogs[pl.ds(r0, BLOCK), :].astype(F32))
        scale = lax.rsqrt(jnp.mean(g * g, axis=-1, keepdims=True) + EPS)
        ng[0, pl.ds(r0, BLOCK), :] = (g * scale * gain).astype(BF16)

        @pl.when(i > 0)
        def _():
            ag_right(i - 1).start()
            ag_left(i - 1).start()

        return 0

    lax.fori_loop(0, BLOCKS, final, 0)
    for j in range(4):
        second_events(1, j)
    ag_right(BLOCKS - 1).start()
    ag_left(BLOCKS - 1).start()
    loads[7].wait()
    loads[8].wait()
    from_partner(0)
    fg = fgain[...]

    def project(g):
        for i in (2 * g, 2 * g + 1):
            ag_right(i).wait_recv()
            ag_forward_right(i).start()
            ag_left(i).wait_recv()
            ag_forward_left(i).start()
        for i in (2 * g, 2 * g + 1):
            ag_forward_right(i).wait_recv()
            ag_forward_left(i).wait_recv()
        r0 = ((g + 2) % 3) * 256

        def tile(n, total):
            n0 = pl.multiple_of(n * 256, 256)
            part = dot(ng[0, pl.ds(r0, 256), :], wof[0, :, :, pl.ds(n0, 256)].reshape(INNER, 256))
            for r in (1, 2, 3):
                part = part + dot(
                    ng[r, pl.ds(r0, 256), :], wof[r, :, :, pl.ds(n0, 256)].reshape(INNER, 256)
                )
            s = (stream[pl.ds(r0, 256), pl.ds(n0, 256)].astype(F32) + part).astype(BF16)
            stream[pl.ds(r0, 256), pl.ds(n0, 256)] = s
            sf = s.astype(F32)
            return total + jnp.sum(sf * sf, axis=-1, keepdims=True)

        total = lax.fori_loop(0, 8, tile, jnp.zeros((256, 1), F32))
        scale = lax.rsqrt(total * (1.0 / WIDTH) + EPS)

        def norm(n, _):
            n0 = pl.multiple_of(n * 256, 256)
            sf = stream[pl.ds(r0, 256), pl.ds(n0, 256)].astype(F32)
            fin[pl.ds(16 + r0, 256), pl.ds(n0, 256)] = (
                sf * scale * fgain[:, pl.ds(n0, 256)]
            ).astype(BF16)
            return 0

        lax.fori_loop(0, 8, norm, 0)

    project(0)
    rim = remote(fin.at[pl.ds(ROWS, 16)], fin.at[pl.ds(0, 16)], hsend.at[3], hrecv.at[3], nxt)
    for j in range(4):
        last_events(1, j)

    @pl.when(sp < 31)
    def _():
        rim.start()

    project(1)
    for j in range(4):
        second_events(2, j)
    project(2)
    for j in range(4):
        last_events(2, j)

    @pl.when(sp > 0)
    def _():
        rim.wait_recv()

    from_partner(1)
    from_partner(2)

    def feed(d, store):
        f0 = pl.multiple_of(d * SHARE, 64)

        def tile(n, _):
            n0 = pl.multiple_of(n * 128, 128)
            w = jnp.concatenate(
                [
                    gvd[:, 0, :, pl.ds(n0, 128)].reshape(WIDTH, 128),
                    gvd[:, 1, :, pl.ds(n0, 128)].reshape(WIDTH, 128),
                ],
                axis=1,
            )
            u = dot(fin[pl.ds(f0, SHARE + 16), :], w).astype(BF16).astype(F32)
            taps = jnp.concatenate(
                [gtap[:, pl.ds(n0, 128)].astype(F32), vtap2[:, pl.ds(n0, 128)].astype(F32)], axis=1
            )
            conv = taps[2:3] * u
            for j in range(2):
                conv = conv + taps[j : j + 1] * pltpu.roll(u, 2 - j, 0)
            conv = conv[16:]
            hid[:, pl.ds(n0, 128)] = (silu(conv[:, :128]) * conv[:, 128:]).astype(BF16)
            return 0

        lax.fori_loop(0, HIDDEN // 128, tile, 0)

        def down(n, _):
            n0 = pl.multiple_of(n * 256, 256)
            w = gvd[pl.ds(n * 4, 4), 2].reshape(256, HIDDEN)
            store(
                n0,
                lax.dot_general(hid[...], w, (((1,), (1,)), ((), ())), preferred_element_type=F32),
            )
            return 0

        lax.fori_loop(0, WIDTH // 256, down, 0)

    def keep(slot):
        def store(n0, value):
            sbuf[slot, :, pl.ds(n0, 256)] = value.astype(BF16)

        return store

    def add(slot, r0, ref):
        def body(n, _):
            n0 = pl.multiple_of(n * 256, 256)
            sbuf[slot, pl.ds(r0, 96), pl.ds(n0, 256)] = (
                sbuf[slot, pl.ds(r0, 96), pl.ds(n0, 256)].astype(F32) + ref[:, pl.ds(n0, 256)].astype(F32)
            ).astype(BF16)
            return 0

        lax.fori_loop(0, 8, body, 0)

    def top(ref):
        return ref.at[pl.ds(0, 96)]

    def bottom(ref):
        return ref.at[pl.ds(96, 96)]

    feed((x + 2) % 4, keep(0))
    qa = remote(top(sbuf.at[0]), ra, qsend.at[0], qrecv.at[0], dev_x(1))
    qb = remote(bottom(sbuf.at[0]), rb, qsend.at[1], qrecv.at[1], dev_x(-1))
    start(qa)
    start(qb)
    feed((x + 1) % 4, keep(1))
    q2 = remote(bottom(sbuf.at[1]), bottom(rl), qsend.at[2], qrecv.at[2], dev_x(1))
    start(q2)
    qa.wait_recv()
    add(1, 0, ra)
    q3 = remote(top(sbuf.at[1]), top(rl), qsend.at[3], qrecv.at[3], dev_x(1))
    start(q3)
    feed((x + 3) % 4, keep(2))
    q4 = remote(top(sbuf.at[2]), top(rr), qsend.at[4], qrecv.at[4], dev_x(-1))
    start(q4)
    qb.wait_recv()
    add(2, 96, rb)
    q5 = remote(bottom(sbuf.at[2]), bottom(rr), qsend.at[5], qrecv.at[5], dev_x(-1))
    start(q5)

    def hold(n0, value):
        own[:, pl.ds(n0, 256)] = value

    feed(x, hold)
    x0 = pl.multiple_of(x * SHARE, 64)
    q2.wait_recv()
    q3.wait_recv()
    q4.wait_recv()
    q5.wait_recv()

    def finish(n, _):
        n0 = pl.multiple_of(n * 256, 256)
        cols = pl.ds(n0, 256)
        out[:, cols] = (
            stream[pl.ds(x0, SHARE), cols].astype(F32)
            + own[:, cols]
            + rl[:, cols].astype(F32)
            + rr[:, cols].astype(F32)
        ).astype(BF16)
        return 0

    lax.fori_loop(0, 8, finish, 0)

    for copy in pending:
        copy.wait_send()
    for i in range(BLOCKS):
        ag_right(i).wait_send()
        ag_left(i).wait_send()
        ag_forward_right(i).wait_send()
        ag_forward_left(i).wait_send()

    @pl.when(sp < 31)
    def _():
        for h in halo:
            h.wait_send()
        rim.wait_send()


def on_device(
    mixer_value_projection,
    write_vectors_projected,
    read_vectors_projected,
    output_gate_projected,
    step_size_scores,
    position_decay_extra,
    step_size_bias,
    head_decay_logarithm,
    value_filter_taps,
    write_filter_taps,
    read_filter_taps,
    gated_group_norm_gain,
    mixer_output_weight,
    residual,
    feedforward_norm_gain,
    feedforward_gate_weight,
    feedforward_value_weight,
    gate_filter_taps,
    single_value_filter_taps,
    feedforward_down_weight,
):
    args = (
        mixer_value_projection,
        write_vectors_projected.T,
        read_vectors_projected.T,
        output_gate_projected,
        step_size_scores.T,
        position_decay_extra.T,
        step_size_bias,
        head_decay_logarithm,
        value_filter_taps,
        jnp.concatenate([write_filter_taps, read_filter_taps], axis=1).T,
        gated_group_norm_gain.reshape(1, INNER),
        mixer_output_weight.reshape(32, 16, WIDTH),
        residual,
        feedforward_norm_gain.reshape(1, WIDTH),
        feedforward_gate_weight,
        feedforward_value_weight,
        gate_filter_taps,
        single_value_filter_taps,
        feedforward_down_weight.T,
    )
    hbm = pl.BlockSpec(memory_space=pl.ANY)
    vmem = pl.BlockSpec(memory_space=pltpu.VMEM)
    smem = pl.BlockSpec(memory_space=pltpu.SMEM)
    specs = [hbm, hbm, hbm, hbm, vmem, vmem, smem, smem, vmem, vmem, vmem, hbm, hbm, vmem, hbm, hbm, vmem, vmem, hbm]
    dma = pltpu.SemaphoreType.DMA
    scratch = [
        pltpu.VMEM((16 + ROWS, INNER), BF16),
        pltpu.VMEM((128, 128 + ROWS), BF16),
        pltpu.VMEM((ROWS, INNER), BF16),
        pltpu.VMEM((BLOCKS, HEADS, BLOCK), F32),
        pltpu.VMEM((BLOCKS, HEADS, BLOCK), F32),
        pltpu.VMEM((BLOCKS, 64, BLOCK), BF16),
        pltpu.VMEM((BLOCKS, BLOCK, 64), BF16),
        pltpu.VMEM((ROWS, INNER), BF16),
        pltpu.VMEM((ROWS, INNER), F32),
        pltpu.VMEM((ROWS, INNER), F32),
        pltpu.VMEM((BLOCKS, 64, INNER), F32),
        pltpu.VMEM((BLOCKS, 1, INNER), F32),
        pltpu.VMEM((64, INNER), F32),
        pltpu.VMEM((1, INNER), F32),
        pltpu.VMEM((96, INNER), BF16),
        pltpu.VMEM((96, INNER), BF16),
        pltpu.VMEM((4, 96, INNER), BF16),
        pltpu.VMEM((4, 96, INNER), BF16),
        pltpu.VMEM((2, 64, INNER), F32),
        pltpu.VMEM((4, ROWS, INNER), BF16),
        pltpu.VMEM((ROWS, WIDTH), BF16),
        pltpu.VMEM((16 + ROWS, WIDTH), BF16),
        pltpu.VMEM((4, 32, 16, WIDTH), BF16),
        pltpu.VMEM((32, 3, 64, HIDDEN), BF16),
        pltpu.VMEM((SHARE, HIDDEN), BF16),
        pltpu.VMEM((3, SHARE, WIDTH), BF16),
        pltpu.VMEM((96, WIDTH), BF16),
        pltpu.VMEM((96, WIDTH), BF16),
        pltpu.VMEM((SHARE, WIDTH), BF16),
        pltpu.VMEM((SHARE, WIDTH), BF16),
        pltpu.VMEM((SHARE, WIDTH), F32),
        dma((9,)),
        dma((4,)),
        dma((4,)),
        dma((3,)),
        dma((3,)),
        dma((7,)),
        dma((7,)),
        dma((3, 36)),
        dma((3, 36)),
        dma((4, BLOCKS)),
        dma((4, BLOCKS)),
        dma((6,)),
        dma((6,)),
    ]
    return pl.pallas_call(
        kernel,
        out_shape=jax.ShapeDtypeStruct((SHARE, WIDTH), BF16),
        in_specs=specs,
        out_specs=vmem,
        scratch_shapes=scratch,
        compiler_params=pltpu.CompilerParams(
            collective_id=0, has_side_effects=True, vmem_limit_bytes=64 * 1024 * 1024 - 65536
        ),
        name="layer",
    )(*args)


def solution(mesh):
    torus = Mesh(mesh.devices.reshape(4, 4, 2, mesh.shape["tp"]), ("sp_0", "sp_1", "sp_2", "tp"))
    in_specs = (
        P(SP, "tp"),
        P(SP, "tp"),
        P(SP, "tp"),
        P(SP, "tp"),
        P(SP, "tp"),
        P(SP, "tp"),
        P("tp"),
        P("tp"),
        P(None, "tp"),
        P(None, "tp"),
        P(None, "tp"),
        P("tp"),
        P("tp", None),
        P(SP, None),
        P(),
        P(SP, "tp"),
        P(SP, "tp"),
        P(None, "tp"),
        P(None, "tp"),
        P("tp", SP),
    )
    return jax.shard_map(
        on_device, mesh=torus, in_specs=in_specs, out_specs=P(SP_TP, None), check_vma=False
    )
```

time: 347 us -> 151 us (0.44)
  Pallas kernels: 0 us -> 147 us
  waiting for transfers between devices: 102 us -> 0 us
  blocking collectives: 90.5 us -> 0 us
  matrix products: 43.1 us -> 0 us
  other arithmetic: 34.8 us -> 0.77 us
  local copies, waits for them, and re-layouts: 36.4 us -> 2.82 us
  starting transfers between devices: 21.6 us -> 0 us
  between operations: 16.8 us -> 0.01 us
    pallas_call x0 -> x1, Pallas kernels: none -> 147 us  [on_device(): pl.pallas_call(kernel, out_shape=jax.ShapeDtypeStruct((SHARE, WIDTH), BF1...]
    reduce_scatter x1 -> x0, waiting for transfers between devices: 64.3 us -> none  [on_device(): lax.psum_scatter(jnp.dot(normed, mixer_output_weight, preferred_element_t...]
    dot_general x8 -> x0, matrix products: 43.1 us -> none  [the longest x1 17.3 us: on_device(): jnp.dot(hidden, lax.all_gather(feedforward_down_weight, SP, axis=1, tiled...]
    all_to_all x1 -> x0, blocking collectives: 40.8 us -> none  [sent_and_summed(): parts = lax.all_to_all(split_up(value, dim, length), axis, 0, 0, tiled=True)]
    all_gather x4 -> x0, blocking collectives: 38.5 us -> none  [entering_2(): pieces = jax.tree.map(lambda part: lax.all_gather(part, axis), running)]
    all_to_all x1 -> x0, waiting for transfers between devices: 36.9 us -> none  [sent_to_all(): lax.all_to_all(jnp.broadcast_to(value[None], (length, *value.shape)), axi...]
    ppermute x5 -> x0, starting transfers between devices: 16.8 us -> none  [from_behind(): return lax.ppermute(value, axis, pairs)]
    convert_element_type x10 -> x0, other arithmetic: 12.7 us -> none  [the longest x5 7.9 us: causal_taps(): padded = jnp.concatenate([previous, current], 0).astype(jnp.float32)]
  transfers between devices with their start and end apart: 9 -> 0, of which waited for: 2 -> 0; matrix products, arithmetic and copies ran while one was open for 16% -> 0% of each run, Pallas kernels for 0% -> 0%
where the time goes in v1:
time: 151 us
  Pallas kernels  147 us (97%)
  local copies, waits for them, and re-layouts  2.82 us (2%)
    pallas_call x1, Pallas kernels, on_device(): pl.pallas_call(kernel, out_shape=jax.ShapeDtypeStruct((SHARE, WIDTH), BF1...  147 us

profile of v1, /device:TPU:1, one launch (start us, length us, event | category | flops | bytes accessed | tf_op | source)
XLA Modules:
  0.0 150.8 jit_solution(13662344983451751913)
XLA Ops:
  0.0 0.8 pad_maximum_fusion
  0.8 0.7 copy.23
  1.5 147.2 %layer.1 = bf16[192,2048]{1,0:T(8,128)(2,1)} custom-call(bf16[768,512]{1,0:T(8,128)(2,1)} %xv.1, bf16[64,768]{1,0:T(8,128)(2,1)} %bitcast.12, bf16[64,768]{1,0:T(8,128)(2,1)} %bitcast.13, bf16[768,512]{1,0:T(8,128)(2,1)} %og.1, f32[8,768]{1,0:T(8,128)} %bitcast.14, f32[8,768]{1,0:T(8,128)} %bitcast.15, f32[8]{0:T(128)} %bias.1, f32[8]{0:T(128)} %hlog.1, ...), custom_call_target="tpu_custom_call" | custom-call | tf_op jit(solution)/shard_map/layer/pallas_call | solution.py:701
  148.7 2.1 %copy.25 = bf16[192,2048]{1,0:T(8,128)(2,1)} copy(bf16[192,2048]{1,0:T(8,128)(2,1)} %layer.1) | data formatting | bytes 1572864

commit v2 on v1

--- a/solution.py
+++ b/solution.py
@@ -24,6 +24,7 @@
 WIDTH = 2048
 HIDDEN = 1408
 SHARE = 192
+PLANE = 1024
 
 
 def silu(v):
@@ -35,12 +36,12 @@
 
 
 def kernel(
-    xv, wrt, rdt, og, sct, ext, bias, hlog, vtap, bctap, ggain, wout, res, fgain, gw, vw, gtap, vtap2, dwt,
+    xv, wrt, rdt, og, sct, ext, bias, hlog, vtap, wtap, rtap, ggain, wout, res, fgain, gw, vw, gtap, vtap2, dwt,
     out,
     xs, bct, ogs, st_s, cum_s, bt_s, c_s, sc_s, ecx_s, ins_s, lb_s, pre_s, stv, plog,
-    m1, r1, r2, r3, inc,
-    ng, stream, fin, wof, gvd, hid, sbuf, ra, rb, rl, rr, own,
-    lsem, hsend, hrecv, xsend, xrecv, ssend, srecv, wsend, wrecv, asend, arecv, qsend, qrecv,
+    m1, r1, r2, r3, exc, inc,
+    ng, stream, fin, wof, gvd, rows, hid, sbuf, ra, rb, rl, rr, own,
+    lsem, vsend, vrecv, hsend, hrecv, xsend, xrecv, ssend, srecv, wsend, wrecv, asend, arecv, qsend, qrecv,
 ):
     z = lax.axis_index("sp_0")
     y = lax.axis_index("sp_1")
@@ -101,7 +102,6 @@
         peers += [dev_x(d), dev_y(d), dev_z(d)]
     for peer in peers:
         pl.semaphore_signal(barrier, inc=1, device_id=peer, device_id_type=MESH)
-    pl.semaphore_wait(barrier, len(peers))
 
     pending = []
 
@@ -115,33 +115,70 @@
         remote(rdt.at[:, pl.ds(ROWS - 128, 128)], bct.at[pl.ds(64, 64), pl.ds(0, 128)], hsend.at[2], hrecv.at[2], nxt),
     ]
 
-    @pl.when(sp < 31)
-    def _():
-        for h in halo:
-            h.start()
-
     @pl.when(sp == 0)
     def _():
         xs[pl.ds(0, 16), :] = jnp.zeros((16, INNER), BF16)
         bct[:, pl.ds(0, 128)] = jnp.zeros((128, 128), BF16)
         fin[pl.ds(0, 16), :] = jnp.zeros((16, WIDTH), BF16)
 
-    for r in (1, 2, 3):
-        start(remote(wout.at[sp], wof.at[r, sp], xsend.at[r - 1], xrecv.at[r - 1], dev_x(-r)))
+    def piece(r):
+        return remote(
+            wout.at[sp, :, pl.ds(0, PLANE)],
+            wof.at[r, sp, :, pl.ds(0, PLANE)],
+            xsend.at[r - 1],
+            xrecv.at[r - 1],
+            dev_x(-r),
+        )
 
     def full(batch, k):
         if batch == 0:
-            return wof.at[pl.ds(1, 3), k]
+            return wof.at[pl.ds(1, 3), k, :, pl.ds(0, PLANE)]
         if batch == 1:
             return gvd.at[k, pl.ds(0, 2)]
         return gvd.at[k, 2]
 
     def half(batch, k, side):
         if batch == 0:
-            return wof.at[pl.ds(1, 3), k, :, pl.ds(1024 * side, 1024)]
+            return wof.at[pl.ds(1, 3), k, :, pl.ds(PLANE // 2 * side, PLANE // 2)]
         if batch == 1:
             return gvd.at[k, side]
         return gvd.at[k, 2, pl.ds(32 * side, 32)]
+
+    right = pl.ds(PLANE, WIDTH - PLANE)
+
+    def slab(r, core):
+        return wof.at[r, pl.ds(pl.multiple_of(16 * core, 16), 16), :, right]
+
+    def slab_half(r, core, side):
+        return wof.at[r, pl.ds(pl.multiple_of(16 * core + 8 * side, 8), 8), :, right]
+
+    own_slab = wout.at[pl.ds(pl.multiple_of(16 * c, 16), 16), :, right]
+    w_right = remote(own_slab, slab(3, c), vsend.at[0], vrecv.at[0], dev_x(1))
+    w_left = remote(own_slab, slab(1, c), vsend.at[1], vrecv.at[1], dev_x(-1))
+    w_fright = remote(slab_half(3, c, 0), slab_half(2, c, 0), vsend.at[2], vrecv.at[2], dev_x(1))
+    w_fleft = remote(slab_half(1, c, 1), slab_half(2, c, 1), vsend.at[3], vrecv.at[3], dev_x(-1))
+
+    def slab_partner(r):
+        return remote(slab(r, c), slab(r, c), vsend.at[3 + r], vrecv.at[3 + r], partner)
+
+    def slab_events():
+        w_right.wait_recv()
+        start(w_fright)
+        start(slab_partner(3))
+        w_left.wait_recv()
+        start(w_fleft)
+        start(slab_partner(1))
+
+    def slab_last():
+        w_fright.wait_recv()
+        w_fleft.wait_recv()
+        start(slab_partner(2))
+
+    def slab_from_partner():
+        for r in (1, 2, 3):
+            remote(
+                slab(r, 1 - c), slab(r, 1 - c), vsend.at[3 + r], vrecv.at[3 + r], partner
+            ).wait_recv()
 
     def send(batch, ref, sem, dev):
         start(remote(ref, ref, wsend.at[batch, sem], wrecv.at[batch, sem], dev))
@@ -159,23 +196,37 @@
         k = item(0, 0)
         send(batch, full(batch, k), 1, dev1(-1))
         send(batch, full(batch, k), 0, dev1(1))
-        second_sends(batch, 0)
+
+    def second_copies(batch, j):
+        ref = full(batch, item(order[j], 0))
+        copies = [
+            remote(ref, ref, wsend.at[batch, 5 + 4 * j], wrecv.at[batch, 5 + 4 * j], dev2(-1)),
+            remote(ref, ref, wsend.at[batch, 4 + 4 * j], wrecv.at[batch, 4 + 4 * j], dev2(1)),
+        ]
+        pending.extend(copies)
+        return copies
 
     def second_sends(batch, j):
-        k = item(order[j], 0)
-        send(batch, full(batch, k), 4 + 4 * j + 1, dev2(-1))
-        send(batch, full(batch, k), 4 + 4 * j, dev2(1))
-        to_partner(batch, k)
-
-    def first_events(batch):
+        for copy in second_copies(batch, j):
+            copy.start()
+        to_partner(batch, item(order[j], 0))
+
+    def first_copies(batch):
         k = item(-1, 0)
-        arrive(batch, full(batch, k), 0)
-        send(batch, half(batch, k, 0), 2, dev1(1))
         k2 = item(1, 0)
-        arrive(batch, full(batch, k2), 1)
-        send(batch, half(batch, k2, 1), 3, dev1(-1))
-        second_sends(batch, 1)
-        second_sends(batch, 2)
+        ref, ref2 = half(batch, k, 0), half(batch, k2, 1)
+        copies = [
+            remote(ref, ref, wsend.at[batch, 2], wrecv.at[batch, 2], dev1(1)),
+            remote(ref2, ref2, wsend.at[batch, 3], wrecv.at[batch, 3], dev1(-1)),
+        ]
+        pending.extend(copies)
+        return copies
+
+    def first_forward(batch, copies):
+        arrive(batch, full(batch, item(-1, 0)), 0)
+        copies[0].start()
+        arrive(batch, full(batch, item(1, 0)), 1)
+        copies[1].start()
 
     def third_event(batch):
         k = item(2, 0)
@@ -204,13 +255,6 @@
     def from_partner(batch):
         for i in range(16):
             arrive(batch, full(batch, 2 * i + 1 - c), 20 + i)
-
-    for i in (3, 4, 5):
-        loads[i].wait()
-    for batch in (1, 2):
-        k = item(0, 0)
-        send(batch, full(batch, k), 1, dev1(-1))
-        send(batch, full(batch, k), 0, dev1(1))
 
     head = lax.broadcasted_iota(jnp.int32, (HEADS, 1), 0)
     bias_c = jnp.zeros((HEADS, 1), F32)
@@ -241,23 +285,15 @@
     loads[0].wait()
     loads[1].wait()
     loads[2].wait()
-
-    @pl.when(sp > 0)
-    def _():
-        for h in halo:
-            h.wait_recv()
-
-    stv[...] = jnp.zeros_like(stv)
-    plog[...] = jnp.zeros_like(plog)
     vt = vtap[...].astype(F32)
-    bt = bctap[...].astype(F32)
+    bt = jnp.concatenate([wtap[...].astype(F32).T, rtap[...].astype(F32).T], axis=0)
 
     def local(b, _):
         r0 = pl.multiple_of(b * BLOCK, BLOCK)
-        rows = xs[pl.ds(r0, BLOCK + 16), :].astype(F32)
-        conv = vt[3:4] * rows
+        vals = xs[pl.ds(r0, BLOCK + 16), :].astype(F32)
+        conv = vt[3:4] * vals
         for j in range(3):
-            conv = conv + vt[j : j + 1] * pltpu.roll(rows, 3 - j, 0)
+            conv = conv + vt[j : j + 1] * pltpu.roll(vals, 3 - j, 0)
         xc = silu(conv[16:]).astype(BF16).astype(F32)
         lanes = bct[:, pl.ds(r0, 2 * BLOCK)].astype(F32)
         conv2 = bt[:, 3:4] * lanes
@@ -276,10 +312,8 @@
         tailed = (scaled.astype(F32) * jnp.exp(last - cumx)).astype(BF16)
         ecx_s[pl.ds(r0, BLOCK), :] = jnp.exp(cumx)
         fresh = dot(wt, tailed)
-        lb_s[b] = stv[...]
-        pre_s[b] = plog[...]
-        stv[...] = stv[...] * jnp.exp(last) + fresh
-        plog[...] = plog[...] + last
+        lb_s[b] = fresh
+        pre_s[b] = last
         return 0
 
     def inner(b, _):
@@ -303,41 +337,85 @@
 
     def put(ref, decay, state):
         ref[pl.ds(0, 64), :] = state.astype(BF16)
-        d = jnp.broadcast_to(decay, (16, INNER))
+        d = jnp.broadcast_to(decay, (16, decay.shape[1]))
         high = d.astype(BF16)
         ref[pl.ds(64, 16), :] = high
         ref[pl.ds(80, 16), :] = (d - high.astype(F32)).astype(BF16)
 
-    def take(ref):
-        decay = ref[pl.ds(64, 16), :].astype(F32) + ref[pl.ds(80, 16), :].astype(F32)
-        return decay[0:1], ref[pl.ds(0, 64), :].astype(F32)
+    def take(ref, cols=slice(None)):
+        decay = ref[pl.ds(64, 16), cols].astype(F32) + ref[pl.ds(80, 16), cols].astype(F32)
+        return decay[0:1], ref[pl.ds(0, 64), cols].astype(F32)
 
     def wait_pieces():
         for r in (1, 2, 3):
-            remote(wout.at[sp], wof.at[r, sp], xsend.at[r - 1], xrecv.at[r - 1], dev_x(-r)).wait_recv()
-
-    lax.fori_loop(0, 3, local, 0)
+            piece(r).wait_recv()
+
+    lax.fori_loop(1, 3, local, 0)
+    pl.semaphore_wait(barrier, len(peers))
+
+    @pl.when(sp < 31)
+    def _():
+        for h in halo:
+            h.start()
+
+    for r in (1, 2, 3):
+        start(piece(r))
+    start(w_right)
+    start(w_left)
+    for i in (3, 4, 5):
+        loads[i].wait()
+    for batch in (1, 2):
+        k = item(0, 0)
+        send(batch, full(batch, k), 1, dev1(-1))
+        send(batch, full(batch, k), 0, dev1(1))
+    lax.fori_loop(3, BLOCKS, local, 0)
+
+    @pl.when(sp > 0)
+    def _():
+        for h in halo:
+            h.wait_recv()
+
+    lax.fori_loop(0, 1, local, 0)
+    state = jnp.zeros((64, INNER), F32)
+    total_log = jnp.zeros((1, INNER), F32)
+    for b in range(BLOCKS):
+        fresh, last = lb_s[b], pre_s[b]
+        lb_s[b] = state
+        pre_s[b] = total_log
+        state = state * jnp.exp(last) + fresh
+        total_log = total_log + last
+    stv[...] = state
+    plog[...] = total_log
+    put(m1, jnp.exp(total_log), state)
     wait_pieces()
     first_sends(0)
-    lax.fori_loop(3, 6, local, 0)
-
-    put(m1, jnp.exp(plog[...]), stv[...])
-    first_events(0)
-    start(remote(m1, r1, ssend.at[0], srecv.at[0], partner))
+    q0 = remote(m1, r1, ssend.at[0], srecv.at[0], partner)
+    start(q0)
     lax.fori_loop(0, 3, inner, 0)
-    remote(m1, r1, ssend.at[0], srecv.at[0], partner).wait_recv()
-    d_own, s_own = jnp.exp(plog[...]), stv[...]
-    d_par, s_par = take(r1)
+    q0.wait_recv()
+
+    mine = pl.ds(pl.multiple_of(c * 256, 256), 256)
+    d_own, s_own = jnp.exp(plog[:, mine]), stv[:, mine]
+    d_par, s_par = take(r1, mine)
     is_first = c == 0
-    chip_d = d_own * d_par
     chip_s = jnp.where(is_first, s_own * d_par + s_par, s_par * d_own + s_own)
-    put(r2.at[y], chip_d, chip_s)
-    third_event(0)
+    put(r2.at[y], d_own * d_par, chip_s)
     for d in (1, 2, 3):
         start(remote(r2.at[y], r2.at[y], ssend.at[d], srecv.at[d], dev_y(d)))
-    lax.fori_loop(3, 6, inner, 0)
-    for j in (0, 1):
-        second_events(0, j)
+    early = second_copies(1, 0)
+    forwards = [first_copies(batch) for batch in range(3)]
+
+    @pl.when(c == 0)
+    def _():
+        for copy in early:
+            copy.start()
+
+    @pl.when(c == 1)
+    def _():
+        for batch in range(3):
+            first_forward(batch, forwards[batch])
+
+    lax.fori_loop(3, BLOCKS, inner, 0)
     for d in (1, 2, 3):
         src = (y + 4 - d) % 4
         remote(r2.at[src], r2.at[src], ssend.at[d], srecv.at[d], dev_y(d)).wait_recv()
@@ -351,29 +429,38 @@
         exc_s = jnp.where(y > i, exc_s * di + si, exc_s)
         exc_d = jnp.where(y > i, exc_d * di, exc_d)
     put(r3.at[z], row_d, row_s)
-    inc[0] = exc_s
-    inc[1] = jnp.broadcast_to(exc_d, (64, INNER))
-    for j in (2, 3):
-        second_events(0, j)
+    exc[0] = exc_s
+    exc[1] = jnp.broadcast_to(exc_d, (64, 256))
     for d in (1, 2, 3):
         start(remote(r3.at[z], r3.at[z], ssend.at[3 + d], srecv.at[3 + d], dev_z(d)))
-    for j in range(4):
-        last_events(0, j)
+
+    @pl.when(c == 1)
+    def _():
+        for copy in early:
+            copy.start()
+
+    @pl.when(c == 0)
+    def _():
+        for batch in range(3):
+            first_forward(batch, forwards[batch])
+
+    slab_events()
     for d in (1, 2, 3):
         src = (z + 4 - d) % 4
         remote(r3.at[src], r3.at[src], ssend.at[3 + d], srecv.at[3 + d], dev_z(d)).wait_recv()
-    acc = jnp.zeros((64, INNER), F32)
+    acc = jnp.zeros((64, 256), F32)
     for i in (0, 1, 2):
         di, si = take(r3.at[i])
         acc = jnp.where(z > i, acc * di + si, acc)
-    acc = acc * inc[1] + inc[0]
+    inc[c] = acc * exc[1] + exc[0]
+    q1 = remote(inc.at[c], inc.at[c], ssend.at[7], srecv.at[7], partner)
+    start(q1)
+    for j in (0, 1, 2):
+        second_sends(0, j)
+    remote(inc.at[1 - c], inc.at[1 - c], ssend.at[7], srecv.at[7], partner).wait_recv()
     d_par, s_par = take(r1)
-    inc[0] = jnp.where(is_first, acc, acc * d_par + s_par)
-
-    for batch in (1, 2):
-        second_sends(batch, 0)
-        first_events(batch)
-        third_event(batch)
+    arrived = jnp.concatenate([inc[0], inc[1]], axis=1)
+    stv[...] = jnp.where(is_first, arrived, arrived * d_par + s_par)
 
     loads[6].wait()
     gain = ggain[...]
@@ -405,14 +492,14 @@
     def final(i, _):
         b = block_of(i)
         r0 = rows_of(i)
-        state = lb_s[b] + inc[0] * jnp.exp(pre_s[b])
+        state = lb_s[b] + stv[...] * jnp.exp(pre_s[b])
         ent = dot(c_s[b], state.astype(BF16))
         m = ins_s[pl.ds(r0, BLOCK), :] + ecx_s[pl.ds(r0, BLOCK), :] * ent
         g = m * silu(ogs[pl.ds(r0, BLOCK), :].astype(F32))
         scale = lax.rsqrt(jnp.mean(g * g, axis=-1, keepdims=True) + EPS)
         ng[0, pl.ds(r0, BLOCK), :] = (g * scale * gain).astype(BF16)
 
-        @pl.when(i > 0)
+        @pl.when((i > 0) & (i < 5))
         def _():
             ag_right(i - 1).start()
             ag_left(i - 1).start()
@@ -420,39 +507,61 @@
         return 0
 
     lax.fori_loop(0, BLOCKS, final, 0)
+    third_event(0)
+
+    def ag_forward(i):
+        ag_right(i).wait_recv()
+        ag_forward_right(i).start()
+        ag_left(i).wait_recv()
+        ag_forward_left(i).start()
+
+    def ag_last(i):
+        ag_forward_right(i).wait_recv()
+        ag_forward_left(i).wait_recv()
+
+    to_partner(1, item(0, 0))
+    second_sends(1, 1)
+    slab_last()
+    ag_forward(0)
+    ag_right(4).start()
+    ag_left(4).start()
     for j in range(4):
-        second_events(1, j)
-    ag_right(BLOCKS - 1).start()
-    ag_left(BLOCKS - 1).start()
+        second_events(0, j)
+    second_sends(1, 2)
+    third_event(1)
+    ag_forward(1)
+    ag_right(5).start()
+    ag_left(5).start()
+    ag_forward(2)
+    for j in range(4):
+        last_events(0, j)
+    second_sends(2, 0)
+    second_sends(2, 1)
+    second_sends(2, 2)
+    third_event(2)
+    second_events(1, 0)
+    ag_forward(3)
     loads[7].wait()
     loads[8].wait()
-    from_partner(0)
-    fg = fgain[...]
 
     def project(g):
-        for i in (2 * g, 2 * g + 1):
-            ag_right(i).wait_recv()
-            ag_forward_right(i).start()
-            ag_left(i).wait_recv()
-            ag_forward_left(i).start()
-        for i in (2 * g, 2 * g + 1):
-            ag_forward_right(i).wait_recv()
-            ag_forward_left(i).wait_recv()
+        ag_last(2 * g)
+        ag_last(2 * g + 1)
         r0 = ((g + 2) % 3) * 256
 
         def tile(n, total):
-            n0 = pl.multiple_of(n * 256, 256)
-            part = dot(ng[0, pl.ds(r0, 256), :], wof[0, :, :, pl.ds(n0, 256)].reshape(INNER, 256))
+            n0 = pl.multiple_of(n * 512, 512)
+            part = dot(ng[0, pl.ds(r0, 256), :], wof[0, :, :, pl.ds(n0, 512)].reshape(INNER, 512))
             for r in (1, 2, 3):
                 part = part + dot(
-                    ng[r, pl.ds(r0, 256), :], wof[r, :, :, pl.ds(n0, 256)].reshape(INNER, 256)
+                    ng[r, pl.ds(r0, 256), :], wof[r, :, :, pl.ds(n0, 512)].reshape(INNER, 512)
                 )
-            s = (stream[pl.ds(r0, 256), pl.ds(n0, 256)].astype(F32) + part).astype(BF16)
-            stream[pl.ds(r0, 256), pl.ds(n0, 256)] = s
+            s = (stream[pl.ds(r0, 256), pl.ds(n0, 512)].astype(F32) + part).astype(BF16)
+            stream[pl.ds(r0, 256), pl.ds(n0, 512)] = s
             sf = s.astype(F32)
             return total + jnp.sum(sf * sf, axis=-1, keepdims=True)
 
-        total = lax.fori_loop(0, 8, tile, jnp.zeros((256, 1), F32))
+        total = lax.fori_loop(0, 4, tile, jnp.zeros((256, 1), F32), unroll=True)
         scale = lax.rsqrt(total * (1.0 / WIDTH) + EPS)
 
         def norm(n, _):
@@ -465,33 +574,41 @@
 
         lax.fori_loop(0, 8, norm, 0)
 
+    slab_from_partner()
+    from_partner(0)
+    second_events(1, 1)
     project(0)
     rim = remote(fin.at[pl.ds(ROWS, 16)], fin.at[pl.ds(0, 16)], hsend.at[3], hrecv.at[3], nxt)
-    for j in range(4):
-        last_events(1, j)
 
     @pl.when(sp < 31)
     def _():
         rim.start()
 
+    ag_forward(4)
+    second_events(1, 2)
+    ag_forward(5)
+    second_events(1, 3)
+    last_events(1, 0)
     project(1)
-    for j in range(4):
-        second_events(2, j)
+    last_events(1, 1)
+    second_events(2, 0)
+    second_events(2, 1)
+    last_events(1, 2)
     project(2)
-    for j in range(4):
-        last_events(2, j)
+    second_events(2, 2)
+    second_events(2, 3)
+    last_events(1, 3)
 
     @pl.when(sp > 0)
     def _():
         rim.wait_recv()
 
     from_partner(1)
-    from_partner(2)
-
-    def feed(d, store):
-        f0 = pl.multiple_of(d * SHARE, 64)
-
-        def tile(n, _):
+
+    def gates(segments):
+        at = [pl.multiple_of(d * SHARE + 96 * side, 32) for d, side in segments]
+
+        def product(n, slot):
             n0 = pl.multiple_of(n * 128, 128)
             w = jnp.concatenate(
                 [
@@ -500,33 +617,55 @@
                 ],
                 axis=1,
             )
-            u = dot(fin[pl.ds(f0, SHARE + 16), :], w).astype(BF16).astype(F32)
+            both = jnp.concatenate([fin[pl.ds(f0, 112), :] for f0 in at], axis=0)
+            rows[slot] = dot(both, w).astype(BF16)
+
+        def gate(n, slot):
+            n0 = pl.multiple_of(n * 128, 128)
+            u = rows[slot].astype(F32)
             taps = jnp.concatenate(
                 [gtap[:, pl.ds(n0, 128)].astype(F32), vtap2[:, pl.ds(n0, 128)].astype(F32)], axis=1
             )
             conv = taps[2:3] * u
             for j in range(2):
                 conv = conv + taps[j : j + 1] * pltpu.roll(u, 2 - j, 0)
-            conv = conv[16:]
+            conv = jnp.concatenate([conv[16:112], conv[128:]], axis=0)
             hid[:, pl.ds(n0, 128)] = (silu(conv[:, :128]) * conv[:, 128:]).astype(BF16)
+
+        def tile(i, _):
+            gate(2 * i, 0)
+            gate(2 * i + 1, 1)
+            product(2 * i + 2, 0)
+            product(2 * i + 3, 1)
             return 0
 
-        lax.fori_loop(0, HIDDEN // 128, tile, 0)
-
+        product(0, 0)
+        product(1, 1)
+        lax.fori_loop(0, 4, tile, 0)
+        gate(8, 0)
+        gate(9, 1)
+        product(10, 0)
+        gate(10, 0)
+
+    def downs(first, end, store):
         def down(n, _):
-            n0 = pl.multiple_of(n * 256, 256)
-            w = gvd[pl.ds(n * 4, 4), 2].reshape(256, HIDDEN)
+            n0 = pl.multiple_of(n * 512, 512)
+            w = gvd[pl.ds(n * 8, 8), 2].reshape(512, HIDDEN)
             store(
                 n0,
                 lax.dot_general(hid[...], w, (((1,), (1,)), ((), ())), preferred_element_type=F32),
             )
             return 0
 
-        lax.fori_loop(0, WIDTH // 256, down, 0)
+        lax.fori_loop(first, end, down, 0, unroll=True)
+
+    def feed(segments, store):
+        gates(segments)
+        downs(0, 4, store)
 
     def keep(slot):
         def store(n0, value):
-            sbuf[slot, :, pl.ds(n0, 256)] = value.astype(BF16)
+            sbuf[slot, :, pl.ds(n0, 512)] = value.astype(BF16)
 
         return store
 
@@ -546,30 +685,44 @@
     def bottom(ref):
         return ref.at[pl.ds(96, 96)]
 
-    feed((x + 2) % 4, keep(0))
-    qa = remote(top(sbuf.at[0]), ra, qsend.at[0], qrecv.at[0], dev_x(1))
-    qb = remote(bottom(sbuf.at[0]), rb, qsend.at[1], qrecv.at[1], dev_x(-1))
-    start(qa)
-    start(qb)
-    feed((x + 1) % 4, keep(1))
-    q2 = remote(bottom(sbuf.at[1]), bottom(rl), qsend.at[2], qrecv.at[2], dev_x(1))
+    gates([((x + 2) % 4, 0), ((x + 2) % 4, 1)])
+    for j in range(4):
+        last_events(2, j)
+    from_partner(2)
+    firsts = []
+    for i in (0, 1):
+        cols = pl.ds(1024 * i, 1024)
+        downs(2 * i, 2 * i + 2, keep(0))
+        qa = remote(
+            sbuf.at[0, pl.ds(0, 96), cols], ra.at[:, cols], qsend.at[2 * i], qrecv.at[2 * i], dev_x(1)
+        )
+        qb = remote(
+            sbuf.at[0, pl.ds(96, 96), cols], rb.at[:, cols], qsend.at[2 * i + 1], qrecv.at[2 * i + 1], dev_x(-1)
+        )
+        start(qa)
+        start(qb)
+        firsts.append((qa, qb))
+    feed([((x + 1) % 4, 1), ((x + 3) % 4, 0)], keep(1))
+    q2 = remote(top(sbuf.at[1]), bottom(rl), qsend.at[4], qrecv.at[4], dev_x(1))
+    q4 = remote(bottom(sbuf.at[1]), top(rr), qsend.at[5], qrecv.at[5], dev_x(-1))
     start(q2)
-    qa.wait_recv()
-    add(1, 0, ra)
-    q3 = remote(top(sbuf.at[1]), top(rl), qsend.at[3], qrecv.at[3], dev_x(1))
+    start(q4)
+    feed([((x + 1) % 4, 0), ((x + 3) % 4, 1)], keep(2))
+    for qa, _ in firsts:
+        qa.wait_recv()
+    add(2, 0, ra)
+    q3 = remote(top(sbuf.at[2]), top(rl), qsend.at[6], qrecv.at[6], dev_x(1))
     start(q3)
-    feed((x + 3) % 4, keep(2))
-    q4 = remote(top(sbuf.at[2]), top(rr), qsend.at[4], qrecv.at[4], dev_x(-1))
-    start(q4)
-    qb.wait_recv()
+    for _, qb in firsts:
+        qb.wait_recv()
     add(2, 96, rb)
-    q5 = remote(bottom(sbuf.at[2]), bottom(rr), qsend.at[5], qrecv.at[5], dev_x(-1))
+    q5 = remote(bottom(sbuf.at[2]), bottom(rr), qsend.at[7], qrecv.at[7], dev_x(-1))
     start(q5)
 
     def hold(n0, value):
-        own[:, pl.ds(n0, 256)] = value
-
-    feed(x, hold)
+        own[:, pl.ds(n0, 512)] = value
+
+    feed([(x, 0), (x, 1)], hold)
     x0 = pl.multiple_of(x * SHARE, 64)
     q2.wait_recv()
     q3.wait_recv()
@@ -636,7 +789,8 @@
         step_size_bias,
         head_decay_logarithm,
         value_filter_taps,
-        jnp.concatenate([write_filter_taps, read_filter_taps], axis=1).T,
+        write_filter_taps,
+        read_filter_taps,
         gated_group_norm_gain.reshape(1, INNER),
         mixer_output_weight.reshape(32, 16, WIDTH),
         residual,
@@ -650,7 +804,7 @@
     hbm = pl.BlockSpec(memory_space=pl.ANY)
     vmem = pl.BlockSpec(memory_space=pltpu.VMEM)
     smem = pl.BlockSpec(memory_space=pltpu.SMEM)
-    specs = [hbm, hbm, hbm, hbm, vmem, vmem, smem, smem, vmem, vmem, vmem, hbm, hbm, vmem, hbm, hbm, vmem, vmem, hbm]
+    specs = [hbm, hbm, hbm, hbm, vmem, vmem, smem, smem, vmem, vmem, vmem, vmem, hbm, hbm, vmem, hbm, hbm, vmem, vmem, hbm]
     dma = pltpu.SemaphoreType.DMA
     scratch = [
         pltpu.VMEM((16 + ROWS, INNER), BF16),
@@ -669,14 +823,16 @@
         pltpu.VMEM((1, INNER), F32),
         pltpu.VMEM((96, INNER), BF16),
         pltpu.VMEM((96, INNER), BF16),
-        pltpu.VMEM((4, 96, INNER), BF16),
-        pltpu.VMEM((4, 96, INNER), BF16),
-        pltpu.VMEM((2, 64, INNER), F32),
+        pltpu.VMEM((4, 96, 256), BF16),
+        pltpu.VMEM((4, 96, 256), BF16),
+        pltpu.VMEM((2, 64, 256), F32),
+        pltpu.VMEM((2, 64, 256), F32),
         pltpu.VMEM((4, ROWS, INNER), BF16),
         pltpu.VMEM((ROWS, WIDTH), BF16),
         pltpu.VMEM((16 + ROWS, WIDTH), BF16),
         pltpu.VMEM((4, 32, 16, WIDTH), BF16),
         pltpu.VMEM((32, 3, 64, HIDDEN), BF16),
+        pltpu.VMEM((2, SHARE + 32, 256), BF16),
         pltpu.VMEM((SHARE, HIDDEN), BF16),
         pltpu.VMEM((3, SHARE, WIDTH), BF16),
         pltpu.VMEM((96, WIDTH), BF16),
@@ -685,18 +841,20 @@
         pltpu.VMEM((SHARE, WIDTH), BF16),
         pltpu.VMEM((SHARE, WIDTH), F32),
         dma((9,)),
+        dma((7,)),
+        dma((7,)),
         dma((4,)),
         dma((4,)),
         dma((3,)),
         dma((3,)),
-        dma((7,)),
-        dma((7,)),
+        dma((8,)),
+        dma((8,)),
         dma((3, 36)),
         dma((3, 36)),
         dma((4, BLOCKS)),
         dma((4, BLOCKS)),
-        dma((6,)),
-        dma((6,)),
+        dma((8,)),
+        dma((8,)),
     ]
     return pl.pallas_call(
         kernel,

time: 151 us -> 110 us (0.73)
  Pallas kernels: 147 us -> 108 us
    pallas_call x1, Pallas kernels: 147 us -> 108 us  [on_device(): pl.pallas_call(kernel, out_shape=jax.ShapeDtypeStruct((SHARE, WIDTH), BF1...]
where the time goes in v2:
time: 110 us
  Pallas kernels  108 us (98%)
  local copies, waits for them, and re-layouts  2.09 us (2%)
    pallas_call x1, Pallas kernels, on_device(): pl.pallas_call(kernel, out_shape=jax.ShapeDtypeStruct((SHARE, WIDTH), BF1...  108 us

profile of v2, /device:TPU:1, one launch (start us, length us, event | category | flops | bytes accessed | tf_op | source)
XLA Modules:
  0.0 109.9 jit_solution(7421828198404112838)
XLA Ops:
  0.0 107.8 %layer.1 = bf16[192,2048]{1,0:T(8,128)(2,1)} custom-call(bf16[768,512]{1,0:T(8,128)(2,1)} %xv.1, bf16[64,768]{1,0:T(8,128)(2,1)} %bitcast.10, bf16[64,768]{1,0:T(8,128)(2,1)} %bitcast.11, bf16[768,512]{1,0:T(8,128)(2,1)} %og.1, f32[8,768]{1,0:T(8,128)} %bitcast.12, f32[8,768]{1,0:T(8,128)} %bitcast.13, f32[8]{0:T(128)} %bias.1, f32[8]{0:T(128)} %hlog.1, ...), custom_call_target="tpu_custom_call" | custom-call | tf_op jit(solution)/shard_map/layer/pallas_call | solution.py:859
  107.9 2.1 %copy.22 = bf16[192,2048]{1,0:T(8,128)(2,1)} copy(bf16[192,2048]{1,0:T(8,128)(2,1)} %layer.1) | data formatting | bytes 1572864

commit v3 on v2

--- a/solution.py
+++ b/solution.py
@@ -276,11 +276,17 @@
         )
 
     def expand(value):
+        parts = []
+        for _ in range(3):
+            part = value.astype(BF16).astype(F32)
+            parts.append(part)
+            value = value - part
+        columns = jnp.concatenate(parts, axis=0).T.astype(BF16)
         spread = (
-            lax.broadcasted_iota(jnp.int32, (HEADS, INNER), 1) // 64
-            == lax.broadcasted_iota(jnp.int32, (HEADS, INNER), 0)
-        ).astype(F32)
-        return jnp.dot(value.T, spread, preferred_element_type=F32, precision=HI)
+            lax.broadcasted_iota(jnp.int32, (3 * HEADS, INNER), 1) // 64
+            == lax.broadcasted_iota(jnp.int32, (3 * HEADS, INNER), 0) % HEADS
+        )
+        return dot(columns, jnp.where(spread, 1.0, 0.0).astype(BF16))
 
     loads[0].wait()
     loads[1].wait()
@@ -387,8 +393,6 @@
     stv[...] = state
     plog[...] = total_log
     put(m1, jnp.exp(total_log), state)
-    wait_pieces()
-    first_sends(0)
     q0 = remote(m1, r1, ssend.at[0], srecv.at[0], partner)
     start(q0)
     lax.fori_loop(0, 3, inner, 0)
@@ -410,10 +414,13 @@
         for copy in early:
             copy.start()
 
+    wait_pieces()
+    first_sends(0)
+
     @pl.when(c == 1)
     def _():
-        for batch in range(3):
-            first_forward(batch, forwards[batch])
+        first_forward(1, forwards[1])
+        first_forward(2, forwards[2])
 
     lax.fori_loop(3, BLOCKS, inner, 0)
     for d in (1, 2, 3):
@@ -441,10 +448,10 @@
 
     @pl.when(c == 0)
     def _():
-        for batch in range(3):
-            first_forward(batch, forwards[batch])
-
-    slab_events()
+        first_forward(1, forwards[1])
+        first_forward(2, forwards[2])
+
+    first_forward(0, forwards[0])
     for d in (1, 2, 3):
         src = (z + 4 - d) % 4
         remote(r3.at[src], r3.at[src], ssend.at[3 + d], srecv.at[3 + d], dev_z(d)).wait_recv()
@@ -455,6 +462,7 @@
     inc[c] = acc * exc[1] + exc[0]
     q1 = remote(inc.at[c], inc.at[c], ssend.at[7], srecv.at[7], partner)
     start(q1)
+    slab_events()
     for j in (0, 1, 2):
         second_sends(0, j)
     remote(inc.at[1 - c], inc.at[1 - c], ssend.at[7], srecv.at[7], partner).wait_recv()
@@ -521,7 +529,6 @@
 
     to_partner(1, item(0, 0))
     second_sends(1, 1)
-    slab_last()
     ag_forward(0)
     ag_right(4).start()
     ag_left(4).start()
@@ -532,15 +539,16 @@
     ag_forward(1)
     ag_right(5).start()
     ag_left(5).start()
+    slab_last()
     ag_forward(2)
     for j in range(4):
         last_events(0, j)
+    second_events(1, 0)
     second_sends(2, 0)
     second_sends(2, 1)
-    second_sends(2, 2)
-    third_event(2)
-    second_events(1, 0)
     ag_forward(3)
+    second_events(1, 1)
+    second_events(1, 2)
     loads[7].wait()
     loads[8].wait()
 
@@ -576,7 +584,6 @@
 
     slab_from_partner()
     from_partner(0)
-    second_events(1, 1)
     project(0)
     rim = remote(fin.at[pl.ds(ROWS, 16)], fin.at[pl.ds(0, 16)], hsend.at[3], hrecv.at[3], nxt)
 
@@ -584,20 +591,21 @@
     def _():
         rim.start()
 
+    second_events(1, 3)
+    second_sends(2, 2)
+    third_event(2)
     ag_forward(4)
-    second_events(1, 2)
     ag_forward(5)
-    second_events(1, 3)
+    second_events(2, 0)
+    project(1)
     last_events(1, 0)
-    project(1)
     last_events(1, 1)
-    second_events(2, 0)
     second_events(2, 1)
+    project(2)
     last_events(1, 2)
-    project(2)
+    last_events(1, 3)
     second_events(2, 2)
     second_events(2, 3)
-    last_events(1, 3)
 
     @pl.when(sp > 0)
     def _():

time: 110 us -> 107 us (0.973)
  Pallas kernels: 108 us -> 105 us
    pallas_call x1, Pallas kernels: 108 us -> 105 us  [on_device(): pl.pallas_call(kernel, out_shape=jax.ShapeDtypeStruct((SHARE, WIDTH), BF1...]
where the time goes in v3:
time: 107 us
  Pallas kernels  105 us (98%)
  local copies, waits for them, and re-layouts  2.09 us (2%)
    pallas_call x1, Pallas kernels, on_device(): pl.pallas_call(kernel, out_shape=jax.ShapeDtypeStruct((SHARE, WIDTH), BF1...  105 us

profile of v3, /device:TPU:1, one launch (start us, length us, event | category | flops | bytes accessed | tf_op | source)
XLA Modules:
  0.0 107.1 jit_solution(9268333848695651593)
XLA Ops:
  0.0 105.0 %layer.1 = bf16[192,2048]{1,0:T(8,128)(2,1)} custom-call(bf16[768,512]{1,0:T(8,128)(2,1)} %xv.1, bf16[64,768]{1,0:T(8,128)(2,1)} %bitcast.10, bf16[64,768]{1,0:T(8,128)(2,1)} %bitcast.11, bf16[768,512]{1,0:T(8,128)(2,1)} %og.1, f32[8,768]{1,0:T(8,128)} %bitcast.12, f32[8,768]{1,0:T(8,128)} %bitcast.13, f32[8]{0:T(128)} %bias.1, f32[8]{0:T(128)} %hlog.1, ...), custom_call_target="tpu_custom_call" | custom-call | tf_op jit(solution)/shard_map/layer/pallas_call | solution.py:867
  105.0 2.1 %copy.22 = bf16[192,2048]{1,0:T(8,128)(2,1)} copy(bf16[192,2048]{1,0:T(8,128)(2,1)} %layer.1) | data formatting | bytes 1572864
